TPU v7x, 256 devices: a whole 4x4x8 slice. The times are simulated.
256 devices in a mesh: sp: 64 (over z, x, core), tp: 4 (over y).
Axes of the slice: x: 4, y: 4, z: 8, core: 2. Of those that a mesh axis runs over, the one named last changes fastest.
Arguments:
- result_cotangent_values: bfloat16 [8192, 2048], P('sp'), may hold values from -16 to 16
- specialist_entry_vectors: bfloat16 [8192, 2048], P('sp'), may hold values from -6 to 6
- chosen_specialists: int32 [8192, 2], P('sp'), may hold values from 0 to 31, all different within a row; in each aligned block of 128 rows (0 to 127, 128 to 255, ...) at most 16 rows name the same one
- specialist_mixing_shares: float32 [8192, 2], P('sp'), may hold values from 0.1 to 0.9
- specialist_switch_maps: bfloat16 [64, 2048, 1792], P('sp', None, 'tp'), may hold values from -0.125 to 0.125
- specialist_widen_maps: bfloat16 [64, 2048, 1792], P('sp', None, 'tp'), may hold values from -0.125 to 0.125
- specialist_shrink_maps: bfloat16 [64, 1792, 2048], P('sp', 'tp'), may hold values from -0.09375 to 0.09375
- memory_readout_map: bfloat16 [2048, 2048], P('sp', 'tp'), may hold values from -0.125 to 0.125
- memory_source_vectors: bfloat16 [8192, 2048], P('sp', 'tp'), may hold values from -6 to 6
- memory_hidden_values: bfloat16 [8192, 2048], P('sp', 'tp'), may hold values from -6 to 6
- feature_fading_speed: float32 [2048], P('tp'), may hold values from 2.03450521e-06 to 0.009
- extra_log_fading: float32 [8192], P('sp'), may hold values from -2.8 to 0
- memory_switch_tiles: bfloat16 [8, 256, 256], P('tp'), may hold values from -0.375 to 0.375
- entry_switch_tiles: bfloat16 [8, 256, 256], P('tp'), may hold values from -0.375 to 0.375
Outputs:
- gate_proj_grad: bfloat16 [64, 2048, 1792], P('sp', None, 'tp')
- up_proj_grad: bfloat16 [64, 2048, 1792], P('sp', None, 'tp')
- down_proj_grad: bfloat16 [64, 1792, 2048], P('sp', 'tp')
- out_proj_grad: float32 [2048, 2048], P('sp', 'tp')
- lru_input_grad: float32 [8192, 2048], P('sp', 'tp')
Inputs may be any that keep to these rules, and one draw needn't show every extreme that they name: `chosen_specialists`: each token names two different experts; among the 128 tokens of one device no expert is named more than 16 times, a bound that some block reaches on some device.
All inputs are finite; a program needn't handle non-finite values.
Results may differ from a plain program's by a relative error of at most 0.009.
Values may be sent and summed in bfloat16 or wider, within the bound.
A program may use at most 128 MiB of HBM per device.

v0:
```python
import functools

import jax
import jax.numpy as jnp
from jax import lax
from jax.experimental import pallas as pl
from jax.experimental.pallas import tpu as pltpu
from jax.sharding import Mesh
from jax.sharding import PartitionSpec as P

SLICES = 2
SP = ("sp_0", "sp_1", "sp_2")
MESH = pl.DeviceIdType.MESH
F32, BF16 = jnp.float32, jnp.bfloat16


def place():
    return tuple(lax.axis_index(n) for n in ("sp_0", "sp_1", "sp_2", "tp"))


def offset_of(k, count):
    odd = lax.rem(k, 2)
    return lax.rem(odd * ((k + 1) // 2) + (1 - odd) * (count - k // 2), count)


def greet_peers(dims, far_share):
    nz, nx, ny = dims
    z, x, c, y = place()
    barrier = pltpu.get_barrier_semaphore()

    def greet(i, _):
        to = (lax.rem(z + i // nx, nz), lax.rem(x + lax.rem(i, nx), nx), c, y)
        pl.semaphore_signal(barrier, inc=1, device_id=to, device_id_type=MESH)
        return 0

    lax.fori_loop(1, nz * nx, greet, 0)
    steps = (1, 2, 3) if far_share else (1, 3)
    for step in steps:
        to = (z, x, c, lax.rem(y + step, ny))
        pl.semaphore_signal(barrier, inc=1, device_id=to, device_id_type=MESH)
    pl.semaphore_signal(barrier, inc=1, device_id=(z, x, 1 - c, y), device_id_type=MESH)
    return barrier, nz * nx - 1 + len(steps) + 1


def drained(ref, sem):
    pltpu.make_async_copy(ref, ref, sem).wait()


def dispatch_kernel(
    dims, cap, target, share, cot, rows, out, slots, own_sem, d_send, d_recv, y_send, y_recv,
    f_send, f_recv, c_send, c_recv,
):
    nz, nx, ny = dims
    z, x, c, y = place()
    barrier, greetings = greet_peers(dims, False)
    width = cot.shape[1] // ny
    half = nz * nx * cap
    group = nx * cap
    cols = pl.ds(pl.multiple_of(y * width, 128), width)

    slot = lax.broadcasted_iota(jnp.int32, (half, target.shape[1]), 0)
    onehot = jnp.where(slot == target[...], 1.0, 0.0).astype(BF16)
    some = rows[:, cols]
    slots[0] = jnp.dot(
        onehot, jnp.concatenate([some, some], axis=0), preferred_element_type=F32
    ).astype(BF16)
    some = cot[:, cols].astype(F32)
    scaled = [(share[:, k : k + 1] * some).astype(BF16) for k in range(2)]
    slots[1] = jnp.dot(
        onehot, jnp.concatenate(scaled, axis=0), preferred_element_type=F32
    ).astype(BF16)

    pl.semaphore_wait(barrier, greetings)

    def source(e):
        return slots.at[:, pl.ds(pl.multiple_of(e * cap, cap), cap), :]

    def target_rows(k):
        start = pl.multiple_of(c * half + (k * nx + x) * cap, cap)
        return out.at[:, pl.ds(start, cap), cols]

    own = pltpu.make_async_copy(source(z * nx + x), target_rows(0), own_sem)
    own.start()

    def push(i, _):
        k, dx = i // nx, lax.rem(i, nx)
        tz, tx = lax.rem(z + offset_of(k, nz), nz), lax.rem(x + dx, nx)
        pltpu.make_async_remote_copy(
            src_ref=source(tz * nx + tx),
            dst_ref=target_rows(k),
            send_sem=d_send,
            recv_sem=d_recv.at[k],
            device_id=(tz, tx, c, y),
            device_id_type=MESH,
        ).start()
        return 0

    lax.fori_loop(1, nz * nx, push, 0)

    def block(k, turn):
        start = pl.multiple_of(c * half + k * group, cap)
        share_of = lax.rem(y + turn, ny)
        return out.at[
            :, pl.ds(start, group), pl.ds(pl.multiple_of(share_of * width, 128), width)
        ]

    def across(k, turn):
        pltpu.make_async_remote_copy(
            src_ref=block(k, turn),
            dst_ref=block(k, turn),
            send_sem=c_send,
            recv_sem=c_recv,
            device_id=(z, x, 1 - c, y),
            device_id_type=MESH,
        ).start()

    def along(k, turn, step, send, recv):
        copy = pltpu.make_async_remote_copy(
            src_ref=block(k, turn),
            dst_ref=block(k, turn),
            send_sem=send,
            recv_sem=recv,
            device_id=(z, x, c, lax.rem(y + step, ny)),
            device_id_type=MESH,
        )
        copy.start()

    for turn in range(nz + 3):
        k = turn
        if k < nz:
            if k == 0:
                drained(slots.at[:, pl.ds(0, group - cap), :], d_recv.at[0])
                own.wait()
            else:
                drained(block(k, 0), d_recv.at[k])
            along(k, 0, 1, y_send.at[0, k], y_recv.at[0, k])
            along(k, 0, 3, y_send.at[1, k], y_recv.at[1, k])
            across(k, 0)
        k = turn - 2
        if 0 <= k < nz:
            drained(block(k, 3), y_recv.at[0, k])
            if k % 2 == 0:
                along(k, 3, 1, f_send.at[k], f_recv.at[k])
            across(k, 3)
            drained(block(k, 1), y_recv.at[1, k])
            if k % 2 == 1:
                along(k, 1, 3, f_send.at[k], f_recv.at[k])
            across(k, 1)
        k = turn - 3
        if 0 <= k < nz:
            drained(block(k, 2), f_recv.at[k])
            across(k, 2)

    whole = out.at[:, pl.ds(pl.multiple_of((1 - c) * half, cap), half), :]
    drained(whole, c_recv)
    drained(whole, c_send)
    drained(slots.at[:, pl.ds(0, half - cap), :], d_send)
    for k in range(nz):
        drained(block(k, 0), y_send.at[0, k])
        drained(block(k, 0), y_send.at[1, k])
        drained(block(k, 2), f_send.at[k])


def dispatched(dims, cap, target, share, cot, rows):
    nz, nx, ny = dims
    half = nz * nx * cap
    vmem = pl.BlockSpec(memory_space=pltpu.VMEM)
    dma = pltpu.SemaphoreType.DMA
    return pl.pallas_call(
        functools.partial(dispatch_kernel, dims, cap),
        out_shape=jax.ShapeDtypeStruct((2, 2 * half, cot.shape[1]), BF16),
        in_specs=[vmem] * 4,
        out_specs=pl.BlockSpec(memory_space=pl.ANY),
        scratch_shapes=[
            pltpu.VMEM((2, half, cot.shape[1] // ny), BF16),
            dma, dma, dma((nz,)), dma((2, nz)), dma((2, nz)), dma((nz,)), dma((nz,)), dma, dma,
        ],
        compiler_params=pltpu.CompilerParams(collective_id=0, has_side_effects=True),
        name="dispatch",
    )(target, share, cot, rows)


def return_kernel(
    dims, cap, part, target, cot, out, pair, sums, far, near, back, mine, moe, own_sem,
    p_send, p_recv, y_send, y_recv, r_send, r_recv, m_send, m_recv,
):
    nz, nx, ny = dims
    z, x, c, y = place()
    barrier, greetings = greet_peers(dims, True)
    width = cot.shape[1] // ny
    half = nz * nx * cap
    mid = half // 2
    pl.semaphore_wait(barrier, greetings)

    def cols(turn):
        return pl.ds(pl.multiple_of(lax.rem(y + turn, ny) * width, 128), width)

    def remote(src, dst, send, recv, to):
        pltpu.make_async_remote_copy(
            src_ref=src, dst_ref=dst, send_sem=send, recv_sem=recv, device_id=to,
            device_id_type=MESH,
        ).start()

    theirs = pl.ds(pl.multiple_of((1 - c) * half, cap), half)
    ours = pl.multiple_of(c * half, cap)
    order = (2, 1, 3, 0)
    for turn in order:
        remote(
            part.at[theirs, cols(turn)], pair.at[turn], p_send.at[turn], p_recv.at[turn],
            (z, x, 1 - c, y),
        )
    up, down = (z, x, c, lax.rem(y + 1, ny)), (z, x, c, lax.rem(y + 3, ny))
    low, high = pl.ds(0, mid), pl.ds(mid, mid)

    def added(turn):
        drained(pair.at[turn], p_recv.at[turn])

        def some(i, _):
            here = pl.multiple_of(i * 64, 64)
            total = part[pl.ds(ours + here, 64), cols(turn)].astype(F32)
            total = total + pair[turn, pl.ds(here, 64), :].astype(F32)
            sums[turn, pl.ds(here, 64), :] = total.astype(BF16)
            return 0

        lax.fori_loop(0, half // 64, some, 0)

    added(2)
    remote(sums.at[2, low], far.at[0], y_send.at[0], y_recv.at[0], up)
    remote(sums.at[2, high], far.at[1], y_send.at[1], y_recv.at[1], down)
    added(1)
    remote(sums.at[1, high], near.at[0, high], y_send.at[2], y_recv.at[2], up)
    added(3)
    remote(sums.at[3, low], near.at[1, low], y_send.at[3], y_recv.at[3], down)
    added(0)

    def joined(side, turn, first):
        drained(far.at[side], y_recv.at[side])

        def some(i, _):
            here = pl.multiple_of(i * 64, 64)
            total = sums[turn, pl.ds(first + here, 64), :].astype(F32)
            total = total + far[side, pl.ds(here, 64), :].astype(F32)
            sums[turn, pl.ds(first + here, 64), :] = total.astype(BF16)
            return 0

        lax.fori_loop(0, mid // 64, some, 0)

    joined(0, 1, 0)
    remote(sums.at[1, low], near.at[0, low], y_send.at[4], y_recv.at[4], up)
    joined(1, 3, mid)
    remote(sums.at[3, high], near.at[1, high], y_send.at[5], y_recv.at[5], down)

    me = z * nx + x

    def finished(first, early, late):
        drained(far.at[0], y_recv.at[early])
        drained(far.at[0], y_recv.at[late])

        def some(i, _):
            here = pl.multiple_of(first + i * 64, 64)
            total = sums[0, pl.ds(here, 64), :].astype(F32)
            total = total + near[0, pl.ds(here, 64), :].astype(F32)
            total = total + near[1, pl.ds(here, 64), :].astype(F32)
            mine[pl.ds(here, 64), :] = total.astype(BF16)
            return 0

        lax.fori_loop(0, mid // 64, some, 0)

    def give(i, _):
        k, sx = i // nx, lax.rem(i, nx)
        sx = lax.rem(x + sx, nx)
        to = (lax.rem(z + nz - offset_of(k, nz), nz), sx, c, y)
        remote(
            mine.at[pl.ds(pl.multiple_of((k * nx + sx) * cap, cap), cap), :],
            back.at[pl.ds(pl.multiple_of(me * cap, cap), cap), :],
            r_send, r_recv, to,
        )
        return 0

    finished(mid, 2, 5)
    lax.fori_loop(nz * nx // 2, nz * nx, give, 0)
    finished(0, 4, 3)
    own = pltpu.make_async_copy(
        mine.at[pl.ds(pl.multiple_of(x * cap, cap), cap), :],
        back.at[pl.ds(pl.multiple_of(me * cap, cap), cap), :],
        own_sem,
    )
    own.start()
    lax.fori_loop(1, nz * nx // 2, give, 0)
    slot = lax.broadcasted_iota(jnp.int32, (cot.shape[0], half), 1)
    chosen = (slot == target[:, 0:1]) | (slot == target[:, 1:2])
    onehot = jnp.where(chosen, 1.0, 0.0).astype(BF16)
    own.wait()
    drained(back.at[pl.ds(0, half - cap), :], r_recv)
    moe[:, cols(0)] = jnp.dot(onehot, back[...], preferred_element_type=F32).astype(BF16)
    for step in (1, 3, 2):
        remote(
            moe.at[:, cols(0)], moe.at[:, cols(0)], m_send.at[step - 1], m_recv.at[step - 1],
            (z, x, c, lax.rem(y + step, ny)),
        )
    for step in (1, 3, 2):
        drained(moe.at[:, cols(ny - step)], m_recv.at[step - 1])
    out[...] = (cot[...].astype(F32) + moe[...].astype(F32)).astype(BF16)

    for turn in range(4):
        drained(pair.at[turn], p_send.at[turn])
    for i in range(6):
        drained(far.at[0], y_send.at[i])
    drained(back.at[pl.ds(0, half - cap), :], r_send)
    for step in (1, 2, 3):
        drained(moe.at[:, cols(0)], m_send.at[step - 1])


def returned(dims, cap, part, target, cot):
    nz, nx, ny = dims
    half, width = nz * nx * cap, cot.shape[1] // ny
    vmem = pl.BlockSpec(memory_space=pltpu.VMEM)
    dma = pltpu.SemaphoreType.DMA
    return pl.pallas_call(
        functools.partial(return_kernel, dims, cap),
        out_shape=jax.ShapeDtypeStruct(cot.shape, BF16),
        in_specs=[vmem] * 3,
        out_specs=vmem,
        scratch_shapes=[
            pltpu.VMEM((4, half, width), BF16),
            pltpu.VMEM((4, half, width), BF16),
            pltpu.VMEM((2, half // 2, width), BF16),
            pltpu.VMEM((2, half, width), BF16),
            pltpu.VMEM((half, width), BF16),
            pltpu.VMEM((half, width), BF16),
            pltpu.VMEM(cot.shape, BF16),
            dma, dma((4,)), dma((4,)), dma((6,)), dma((6,)), dma, dma, dma((3,)), dma((3,)),
        ],
        compiler_params=pltpu.CompilerParams(collective_id=1, has_side_effects=True),
        name="give_back",
    )(part, target, cot)


def joined_along(blocks, dim):
    dims = list(blocks.shape[1:])
    dims[dim] *= blocks.shape[0]
    return jnp.moveaxis(blocks, 0, dim).reshape(dims)


def copy_for_each(shard, axis):
    copies = jnp.broadcast_to(shard, (lax.axis_size(axis), *shard.shape))
    return lax.all_to_all(copies, axis, split_axis=0, concat_axis=0, tiled=True)


def stacked_from(shard, axes, turns):
    blocks = shard
    for k in turns:
        blocks = lax.all_gather(blocks, axes[k])
    done = turns[::-1]
    back = [done.index(k) for k in range(len(axes))]
    blocks = blocks.transpose(*back, *range(len(axes), blocks.ndim))
    return blocks.reshape(-1, *shard.shape)


def gather_axes(shard, axes, turns, dim):
    return joined_along(stacked_from(shard, axes, turns), dim)


def gathered_once(shard, axis):
    leaves = jax.tree.leaves(shard)
    turns = sorted(range(len(leaves)), key=lambda k: -leaves[k].size)
    width = (1, *leaves[turns[0]].shape)[-1]
    lines = [
        jnp.pad(leaves[k].reshape(-1), (0, -leaves[k].size % width)).reshape(-1, width)
        for k in turns
    ]
    both, at, found = (copy_for_each(jnp.concatenate(lines), axis), 0, {})
    for k, line in zip(turns, lines):
        slab = both[:, at : at + len(line)].reshape(len(both), -1)
        found[k] = slab[:, : leaves[k].size].reshape(-1, *leaves[k].shape)
        at += len(line)
    numbers = iter(range(len(leaves)))
    return jax.tree.map(lambda _: found[next(numbers)], shard)


def joined_by_halves(pieces, combine):
    while len(jax.tree.leaves(pieces)[0]) > 1:
        pieces = jax.vmap(combine)(
            *(jax.tree.map(lambda part: part[side::2], pieces) for side in (0, 1))
        )
    return jax.tree.map(lambda part: part[0], pieces)


def entering(shard, axis, combine, identity):
    length, mine = (lax.axis_size(axis), lax.axis_index(axis))
    passed = jnp.arange(length) > mine

    def kept(part, zero, own):
        part = jnp.where(
            passed.reshape(-1, *(1 for _ in own.shape)), part, jnp.asarray(zero, own.dtype)
        )
        return part[::-1]

    pieces = gathered_once(shard, axis)
    return joined_by_halves(jax.tree.map(kept, pieces, identity, shard), combine)


def in_blocks(shard, dim, length):
    before, after = (shard.shape[:dim], shard.shape[dim + 1 :])
    return jnp.moveaxis(shard.reshape(*before, length, -1, *after), dim, 0)


def sent_and_summed(shard, axis, dim):
    blocks = in_blocks(shard, dim, lax.axis_size(axis))
    arrived = lax.all_to_all(blocks, axis, split_axis=0, concat_axis=0, tiled=True)
    return arrived.astype(jnp.float32).sum(axis=0)


def silu_slope(value):
    sig_value = jax.nn.sigmoid(value)
    return sig_value * (1.0 + value * (1.0 - sig_value))


def compose(upper_map, lower_map):
    return (lower_map[0] * upper_map[0], lower_map[1] + lower_map[0] * upper_map[1])


def chain_join(higher_map, lower_map):
    return (lower_map[0] * higher_map[0], lower_map[1] + lower_map[0] * higher_map[1])


def expert_backward(inputs, grads_in, gate_weight, up_weight, down_weight):
    gate_value = jnp.dot(inputs, gate_weight, preferred_element_type=jnp.float32)
    up_value = jnp.dot(inputs, up_weight, preferred_element_type=jnp.float32)
    active = jax.nn.silu(gate_value)
    hidden = (active * up_value).astype(jnp.bfloat16)
    down_grad = jnp.einsum(
        "rf,rd->fd", hidden, grads_in, preferred_element_type=jnp.float32
    ).astype(jnp.bfloat16)
    hidden_grad = jnp.einsum("rd,fd->rf", grads_in, down_weight, preferred_element_type=jnp.float32)
    gate_grad = (hidden_grad * up_value * silu_slope(gate_value)).astype(jnp.bfloat16)
    up_grad = (hidden_grad * active).astype(jnp.bfloat16)
    gate_weight_grad = jnp.einsum(
        "rd,rf->df", inputs, gate_grad, preferred_element_type=jnp.float32
    ).astype(jnp.bfloat16)
    up_weight_grad = jnp.einsum(
        "rd,rf->df", inputs, up_grad, preferred_element_type=jnp.float32
    ).astype(jnp.bfloat16)
    token_part = jnp.einsum("rf,df->rd", gate_grad, gate_weight, preferred_element_type=jnp.float32)
    token_part = token_part + jnp.einsum(
        "rf,df->rd", up_grad, up_weight, preferred_element_type=jnp.float32
    )
    return (gate_weight_grad, up_weight_grad, down_grad, token_part)


def local(
    result_cotangent_values,
    specialist_entry_vectors,
    chosen_specialists,
    specialist_mixing_shares,
    specialist_switch_maps,
    specialist_widen_maps,
    specialist_shrink_maps,
    memory_readout_map,
    memory_source_vectors,
    memory_hidden_values,
    feature_fading_speed,
    extra_log_fading,
    memory_switch_tiles,
    entry_switch_tiles,
):
    tok_rows, feature_count = result_cotangent_values.shape
    route_count = chosen_specialists.shape[1]
    sp_count = lax.axis_size(SP)
    expert_count = sp_count // SLICES
    capacity = min(tok_rows, 4 * tok_rows // expert_count)
    pairs = chosen_specialists.T.reshape(-1)
    order = (jnp.arange(tok_rows)[None, :] * route_count + jnp.arange(route_count)[:, None]).reshape(-1)
    earlier = (pairs[:, None] == pairs[None, :]) & (order[:, None] < order[None, :])
    target = pairs * capacity + jnp.sum(earlier.astype(jnp.int32), axis=0)
    dims = (lax.axis_size("sp_0"), lax.axis_size("sp_1"), lax.axis_size("tp"))
    both = dispatched(
        dims,
        capacity,
        target[None, :],
        specialist_mixing_shares,
        result_cotangent_values,
        specialist_entry_vectors,
    )
    gate_weight_grad, up_weight_grad, down_grad, token_part = expert_backward(
        both[0],
        both[1],
        specialist_switch_maps[0],
        specialist_widen_maps[0],
        specialist_shrink_maps[0],
    )
    mixed_grad = returned(
        dims,
        capacity,
        token_part.astype(jnp.bfloat16),
        target.reshape(route_count, tok_rows).T,
        result_cotangent_values,
    )
    col_count = memory_readout_map.shape[1]
    columns = mixed_grad
    upstream = jnp.dot(
        columns,
        gather_axes(memory_readout_map, (("sp_0", "sp_1"), "sp_2"), (0, 1), 0),
        preferred_element_type=jnp.float32,
    )
    blocks_here = memory_switch_tiles.shape[0]
    block_width = memory_switch_tiles.shape[1]
    blocks_in = memory_source_vectors.reshape(tok_rows, blocks_here, block_width)
    memory_switch_fraction = jax.nn.sigmoid(
        jnp.einsum(
            "tnc,ncd->tnd", blocks_in, memory_switch_tiles, preferred_element_type=jnp.float32
        ).reshape(tok_rows, col_count)
    )
    inp_open = jax.nn.sigmoid(
        jnp.einsum(
            "tnc,ncd->tnd", blocks_in, entry_switch_tiles, preferred_element_type=jnp.float32
        ).reshape(tok_rows, col_count)
    )
    xin = memory_source_vectors.astype(jnp.float32)
    log_fading_factor = (
        -8.0 * memory_switch_fraction * feature_fading_speed[None, :] + extra_log_fading[:, None]
    )
    decay_mult = jnp.exp(log_fading_factor)
    spare_room = -jnp.expm1(2.0 * log_fading_factor)
    in_scale = jnp.sqrt(jnp.maximum(spare_room, 0.01))
    drive = in_scale * inp_open * xin
    coeff = jnp.concatenate([decay_mult[1:], jnp.ones((1, col_count), jnp.float32)], axis=0)
    prod_after, local_part = lax.associative_scan(compose, (coeff, upstream), reverse=True, axis=0)
    alpha_part = decay_mult[0] * local_part[0]
    beta_part = decay_mult[0] * prod_after[0]
    carried = entering(
        (beta_part, alpha_part),
        SP,
        chain_join,
        (jnp.ones_like(beta_part), jnp.zeros_like(alpha_part)),
    )
    incoming = carried[1]
    dstate = local_part + prod_after * incoming[None, :]
    scale_slope = jnp.where(spare_room > 0.01, -decay_mult * decay_mult / in_scale, 0.0)
    log_grad = dstate * (
        memory_hidden_values.astype(jnp.float32) - drive + scale_slope * inp_open * xin
    )
    grad_rec = (
        log_grad
        * (-8.0 * feature_fading_speed[None, :])
        * memory_switch_fraction
        * (1.0 - memory_switch_fraction)
    ).astype(jnp.bfloat16)
    grad_in = (dstate * in_scale * xin * inp_open * (1.0 - inp_open)).astype(jnp.bfloat16)
    back_rec = jnp.einsum(
        "tnd,ncd->tnc",
        grad_rec.reshape(tok_rows, blocks_here, block_width),
        memory_switch_tiles,
        preferred_element_type=jnp.float32,
    )
    back_in = jnp.einsum(
        "tnd,ncd->tnc",
        grad_in.reshape(tok_rows, blocks_here, block_width),
        entry_switch_tiles,
        preferred_element_type=jnp.float32,
    )
    lru_input_grad = (
        dstate * in_scale * inp_open
        + back_rec.reshape(tok_rows, col_count)
        + back_in.reshape(tok_rows, col_count)
    )
    columns = mixed_grad
    out_proj_grad = sent_and_summed(
        jnp.einsum(
            "tr,tc->rc", columns, memory_hidden_values, preferred_element_type=jnp.float32
        ).astype(jnp.bfloat16),
        SP,
        0,
    )
    return (
        gate_weight_grad[None],
        up_weight_grad[None],
        down_grad[None],
        out_proj_grad,
        lru_input_grad,
    )


def solution(mesh):
    finer = Mesh(mesh.devices.reshape(8, 4, 2, mesh.shape["tp"]), ("sp_0", "sp_1", "sp_2", "tp"))
    in_specs = (
        P(SP, None),
        P(SP, None),
        P(SP, None),
        P(SP, None),
        P(SP, None, "tp"),
        P(SP, None, "tp"),
        P(SP, "tp", None),
        P(SP, "tp"),
        P(SP, "tp"),
        P(SP, "tp"),
        P("tp"),
        P(SP),
        P("tp", None, None),
        P("tp", None, None),
    )
    out_specs = (P(SP, None, "tp"), P(SP, None, "tp"), P(SP, "tp", None), P(SP, "tp"), P(SP, "tp"))
    return jax.shard_map(local, mesh=finer, in_specs=in_specs, out_specs=out_specs, check_vma=False)
```

profile of v0, /device:TPU:1, one launch (start us, length us, event | category | flops | bytes accessed | tf_op | source)
XLA Modules:
  0.0 242.7 jit_solution(3783680911154808253)
XLA Ops:
  7.2 0.7 all-gather.5.cloned.1.call-update
  7.9 0.8 copy.96
  8.8 0.2 convert_reduce_fusion.1
  9.0 0.1 copy.101
  9.1 0.6 add_bitcast_fusion
  9.8 1.4 copy.100.share
  11.2 0.6 add.251.target
  11.8 59.5 %dispatch.1 = bf16[2,1024,2048]{2,1,0:T(8,128)(2,1)} custom-call(s32[1,256]{1,0:T(1,128)} %add.251.target, f32[128,2]{1,0:T(8,128)} %copy.100.share, bf16[128,2048]{1,0:T(8,128)(2,1)} %cot.3, bf16[128,2048]{1,0:T(8,128)(2,1)} %rows.1), custom_call_target="tpu_custom_call" | custom-call | tf_op jit(solution)/shard_map/dispatch/pallas_call | solution.py:169
  71.3 4.4 %fusion.8 = f32[1024,448]{0,1:T(8,128)S(1)} fusion(bf16[2,1024,2048]{2,1,0:T(8,128)(2,1)} %dispatch.1, bf16[1,2048,448]{1,2,0:T(8,128)(2,1)S(1)} %copy-done), kind=kOutput, calls=%fused_computation.9 | convolution fusion | flops 1879048192 | bytes 7864320 | tf_op jit(solution)/shard_map/dot_general | solution.py:428
  75.8 0.2 copy-done.1
  76.0 0.5 copy-done.13
  76.5 2.1 fusion.10
  78.7 2.6 %multiply_convert_fusion.1 = (bf16[1024,448]{0,1:T(8,128)(2,1)S(1)}, bf16[1024,448]{0,1:T(8,128)(2,1)S(1)}) fusion(f32[1024,448]{0,1:T(8,128)S(1)} %fusion.8, f32[1024,448]{0,1:T(8,128)S(1)} %fusion.10, bf16[1,448,2048]{2,1,0:T(8,128)(2,1)S(1)} %copy-done.12, bf16[2,1024,2048]{2,1,0:T(8,128)(2,1)S(1)} %copy-done.1), kind=kOutput, calls=%fused_computation.34 | convolution fusion | flops 1885011968 | bytes 11534336 | tf_op jit(solution)/shard_map/rd,fd->rf/dot_general | solution.py:435
  81.3 2.4 fusion.36
  83.7 4.5 %add_convert_fusion.part = bf16[1024,2048]{1,0:T(8,128)(2,1)} fusion(f32[1024,2048]{1,0:T(8,128)S(1)} %fusion.36, bf16[1024,448]{0,1:T(8,128)(2,1)S(1)} %get-tuple-element.7, bf16[1,2048,448]{1,2,0:T(8,128)(2,1)S(1)} %copy-done.13), kind=kOutput, calls=%fused_computation | convolution fusion | flops 1883242496 | bytes 15335424 | tf_op jit(solution)/shard_map/rf,df->rd/dot_general | solution.py:445
  88.2 48.1 %give_back.1 = bf16[128,2048]{1,0:T(8,128)(2,1)} custom-call(bf16[1024,2048]{1,0:T(8,128)(2,1)} %add_convert_fusion.part, s32[128,2]{1,0:T(8,128)} %get-tuple-element.24.target, bf16[128,2048]{1,0:T(8,128)(2,1)} %cot.3), custom_call_target="tpu_custom_call" | custom-call | tf_op jit(solution)/shard_map/give_back/pallas_call | solution.py:319
  136.3 3.2 %convolution_convert_fusion = bf16[2048,512]{1,0:T(8,128)(2,1)} fusion(bf16[128,2048]{1,0:T(8,128)(2,1)} %give_back.1, bf16[128,512]{1,0:T(8,128)(2,1)S(1)} %copy-done.4), kind=kOutput, calls=%fused_computation.16 | convolution fusion | flops 269484032 | bytes 2752512 | tf_op jit(solution)/shard_map/tr,tc->rc/dot_general | solution.py:569
  139.5 12.7 %all-to-all-start = ((bf16[64,32,512]{2,1,0:T(8,128)(2,1)}), bf16[64,32,512]{2,1,0:T(8,128)(2,1)}, u32[]{:S(2)}, u32[]{:S(2)}) async-start(bf16[64,32,512]{2,1,0:T(8,128)(2,1)} %bitcast.116), calls=%async_computation | async-start | bytes 4194304 | tf_op jit(solution)/shard_map/all_to_all | solution.py:410
  152.3 0.3 fusion.48
  152.6 0.1 copy.116
  152.7 0.2 copy-done.10
  153.0 0.1 fusion.63
  153.1 0.7 copy-done.3
  153.8 0.1 slice.335
  153.9 0.1 slice.339
  154.0 0.1 slice.345
  154.2 0.2 slice.336
  154.3 0.1 slice.340
  154.5 0.1 slice.346
  154.6 5.9 %fusion.30 = bf16[1,2048,448]{1,2,0:T(8,128)(2,1)} fusion(bf16[1024,448]{0,1:T(8,128)(2,1)} %copy-done.14, bf16[2,1024,2048]{2,1,0:T(8,128)(2,1)} %dispatch.1), kind=kOutput, calls=%fused_computation.25 | convolution fusion | flops 1879965696 | bytes 6946816 | tf_op jit(solution)/shard_map/rd,rf->df/dot_general | solution.py:438
  160.5 5.6 %fusion.33 = bf16[1,2048,448]{1,2,0:T(8,128)(2,1)} fusion(bf16[1024,448]{0,1:T(8,128)(2,1)S(1)} %copy-done.16, bf16[2,1024,2048]{2,1,0:T(8,128)(2,1)} %dispatch.1), kind=kOutput, calls=%fused_computation.26 | convolution fusion | flops 1879965696 | bytes 6946816 | tf_op jit(solution)/shard_map/rd,rf->df/dot_general | solution.py:441
  166.2 3.3 %fusion.27 = bf16[1,448,2048]{2,1,0:T(8,128)(2,1)} fusion(bf16[2,1024,2048]{2,1,0:T(8,128)(2,1)S(1)} %bitcast.115, f32[1024,448]{0,1:T(8,128)S(1)} %copy-done.20, f32[1024,448]{0,1:T(8,128)S(1)} %copy-done.18), kind=kOutput, calls=%fused_computation.24 | convolution fusion | flops 1882718208 | bytes 9699328 | tf_op jit(solution)/shard_map/rf,rd->fd/dot_general | solution.py:432
  169.5 0.4 all-gather.7.cloned.1.call-done
  170.0 1.9 copy.102
  171.9 0.4 fusion.98
  172.3 0.1 slice.337
  172.4 0.1 slice.341
  172.5 0.1 slice.338
  172.7 0.1 slice.342
  173.6 0.1 slice.332
  174.6 0.2 slice.333
  175.2 0.7 add_multiply_fusion.11
  175.9 25.9 %all-to-all-done = bf16[64,32,512]{2,1,0:T(8,128)(2,1)} async-done(((bf16[64,32,512]{2,1,0:T(8,128)(2,1)}), bf16[64,32,512]{2,1,0:T(8,128)(2,1)}, u32[]{:S(2)}, u32[]{:S(2)}) %all-to-all-start) | async-done | bytes 2097184 | tf_op jit(solution)/shard_map/all_to_all | solution.py:410
  201.8 0.8 broadcast_in_dim.47
  202.6 7.2 %all-to-all-start.1 = ((f32[64,2,512]{2,1,0:T(2,128)}), f32[64,2,512]{2,1,0:T(2,128)}, u32[]{:S(2)}, u32[]{:S(2)}) async-start(f32[64,2,512]{2,1,0:T(2,128)} %broadcast_in_dim.47), calls=%async_computation.1 | async-start | bytes 524288 | tf_op jit(solution)/shard_map/all_to_all | solution.py:347
  209.7 1.9 fusion.45
  211.7 1.1 copy.117
  212.8 2.5 %convert_reduce_fusion = f32[32,512]{1,0:T(8,128)} fusion(bf16[64,32,512]{2,1,0:T(8,128)(2,1)} %all-to-all-done), kind=kLoop, calls=%fused_computation.13 | loop fusion | flops 2080768 | bytes 2162688 | tf_op jit(solution)/shard_map/reduce_sum | solution.py:411
  215.3 0.7 add.279
  216.1 1.7 rev.4
  217.9 0.1 rev.5
  218.0 4.7 %all-to-all-done.1 = f32[64,2,512]{2,1,0:T(2,128)} async-done(((f32[64,2,512]{2,1,0:T(2,128)}), f32[64,2,512]{2,1,0:T(2,128)}, u32[]{:S(2)}, u32[]{:S(2)}) %all-to-all-start.1) | async-done | bytes 262176 | tf_op jit(solution)/shard_map/all_to_all | solution.py:347
  222.7 1.3 fusion.86
  224.0 0.1 bitcast_select_fusion
  224.1 0.6 slice.408
  224.7 0.6 slice.413
  225.4 1.5 slice.409
  226.9 2.6 %slice.414 = f32[32,512]{1,0:T(8,128)} reverse(f32[32,512]{1,0:T(8,128)} %slice.413), dimensions={0} | reverse | bytes 131072 | tf_op jit(solution)/shard_map/slice | solution.py:384
  229.6 1.2 slice.406
  230.9 0.9 fusion.88
  232.2 1.4 fusion.59
  233.6 0.2 convolution_bitcast_fusion
  233.9 1.2 convolution_bitcast_fusion.1
  235.1 0.8 add_add_fusion
  (179 shorter events, 2.6 us)
Async XLA Ops:
  7.2 64.1 %copy-start = (bf16[1,2048,448]{1,2,0:T(8,128)(2,1)S(1)}, bf16[1,2048,448]{1,2,0:T(8,128)(2,1)}, u32[]{:S(2)}) copy-start(bf16[1,2048,448]{1,2,0:T(8,128)(2,1)} %param.18) | copy-start | bytes 5505028
  7.2 145.7 %all-gather.5.cloned.1.call-start = ((), (), s32[]{:S(2)}) async-start(), calls=%async_computation.2 | async-start | bytes 1081344 | tf_op jit(solution)/shard_map/all_gather | solution.py:353
  71.3 4.7 %copy-start.1 = (bf16[2,1024,2048]{2,1,0:T(8,128)(2,1)S(1)}, bf16[2,1024,2048]{2,1,0:T(8,128)(2,1)}, u32[]{:S(2)}) copy-start(bf16[2,1024,2048]{2,1,0:T(8,128)(2,1)} %dispatch.1) | copy-start | bytes 25165828
  71.3 5.2 %copy-start.13 = (bf16[1,2048,448]{1,2,0:T(8,128)(2,1)S(1)}, bf16[1,2048,448]{1,2,0:T(8,128)(2,1)}, u32[]{:S(2)}) copy-start(bf16[1,2048,448]{1,2,0:T(8,128)(2,1)} %param.19) | copy-start | bytes 5505028
  76.5 2.1 copy-start.17
  76.5 2.2 copy-start.12
  78.7 2.6 %copy-start.19 = (f32[1024,448]{0,1:T(8,128)}, f32[1024,448]{0,1:T(8,128)S(1)}, u32[]{:S(2)}) copy-start(f32[1024,448]{0,1:T(8,128)S(1)} %fusion.10) | copy-start | bytes 5505028
  81.3 2.4 copy-start.14
  81.3 2.4 copy-start.15
  88.2 48.1 %copy-start.4 = (bf16[128,512]{1,0:T(8,128)(2,1)S(1)}, bf16[128,512]{1,0:T(8,128)(2,1)}, u32[]{:S(2)}) copy-start(bf16[128,512]{1,0:T(8,128)(2,1)} %param.23) | copy-start | bytes 393220
  139.5 12.7 %copy-start.7 = (bf16[2,256,256]{2,1,0:T(8,128)(2,1)S(1)}, bf16[2,256,256]{2,1,0:T(8,128)(2,1)}, u32[]{:S(2)}) copy-start(bf16[2,256,256]{2,1,0:T(8,128)(2,1)} %param.26) | copy-start | bytes 786436
  139.5 12.7 %copy-start.8 = (bf16[128,512]{1,0:T(8,128)(2,1)S(1)}, bf16[128,512]{1,0:T(8,128)(2,1)}, u32[]{:S(2)}) copy-start(bf16[128,512]{1,0:T(8,128)(2,1)} %param.22) | copy-start | bytes 393220
  139.5 62.3 %all-to-all-start = ((bf16[64,32,512]{2,1,0:T(8,128)(2,1)}), bf16[64,32,512]{2,1,0:T(8,128)(2,1)}, u32[]{:S(2)}, u32[]{:S(2)}) async-start(bf16[64,32,512]{2,1,0:T(8,128)(2,1)} %bitcast.116), calls=%async_computation | async-start | bytes 4194304 | tf_op jit(solution)/shard_map/all_to_all | solution.py:410
  152.2 0.7 copy-start.10
  152.2 0.8 copy-start.11
  152.2 17.8 %all-gather.7.cloned.1.call-start = ((), (), s32[]{:S(2)}) async-start(), calls=%async_computation.3 | async-start | bytes 3145728 | tf_op jit(solution)/shard_map/all_gather | solution.py:353
  153.1 0.7 copy-start.3
  154.6 5.9 %copy-start.16 = (bf16[1024,448]{0,1:T(8,128)(2,1)S(1)}, bf16[1024,448]{0,1:T(8,128)(2,1)}, u32[]{:S(2)}) copy-start(bf16[1024,448]{0,1:T(8,128)(2,1)} %copy-done.15) | copy-start | bytes 2752516
  154.6 11.6 %slice-start = ((s8[8388608]{0:T(1024)(128)(4,1)}), s8[4194304]{0:T(1024)(128)(4,1)S(1)}, s32[]{:S(2)}) async-start(s8[8388608]{0:T(1024)(128)(4,1)} %bitcast.114), calls=%async_computation.4 | async-start | bytes 8388608
  160.5 5.7 %slice-start.1 = ((s8[8388608]{0:T(1024)(128)(4,1)}), s8[4194304]{0:T(1024)(128)(4,1)S(1)}, s32[]{:S(2)}) async-start(s8[8388608]{0:T(1024)(128)(4,1)} %bitcast.114), calls=%async_computation.5 | async-start | bytes 8388608
  160.5 5.7 %copy-start.18 = (f32[1024,448]{0,1:T(8,128)S(1)}, f32[1024,448]{0,1:T(8,128)}, u32[]{:S(2)}) copy-start(f32[1024,448]{0,1:T(8,128)} %copy-done.17) | copy-start | bytes 5505028
  160.5 5.7 %copy-start.20 = (f32[1024,448]{0,1:T(8,128)S(1)}, f32[1024,448]{0,1:T(8,128)}, u32[]{:S(2)}) copy-start(f32[1024,448]{0,1:T(8,128)} %copy-done.19) | copy-start | bytes 5505028
  170.0 1.9 copy-start.2
  174.9 34.8 %copy-start.9 = (bf16[128,512]{1,0:T(8,128)(2,1)S(1)}, bf16[128,512]{1,0:T(8,128)(2,1)}, u32[]{:S(2)}) copy-start(bf16[128,512]{1,0:T(8,128)(2,1)} %param.22) | copy-start | bytes 393220
  202.6 20.1 %all-to-all-start.1 = ((f32[64,2,512]{2,1,0:T(2,128)}), f32[64,2,512]{2,1,0:T(2,128)}, u32[]{:S(2)}, u32[]{:S(2)}) async-start(f32[64,2,512]{2,1,0:T(2,128)} %broadcast_in_dim.47), calls=%async_computation.1 | async-start | bytes 524288 | tf_op jit(solution)/shard_map/all_to_all | solution.py:347
  217.9 14.3 %copy-start.5 = (bf16[128,512]{1,0:T(8,128)(2,1)S(1)}, bf16[128,512]{1,0:T(8,128)(2,1)}, u32[]{:S(2)}) copy-start(bf16[128,512]{1,0:T(8,128)(2,1)} %param.23) | copy-start | bytes 393220
  225.4 8.2 %copy-start.6 = (bf16[2,256,256]{2,1,0:T(8,128)(2,1)S(1)}, bf16[2,256,256]{2,1,0:T(8,128)(2,1)}, u32[]{:S(2)}) copy-start(bf16[2,256,256]{2,1,0:T(8,128)(2,1)} %param.27) | copy-start | bytes 786436
Sparse Core Ops, SparseCore 0:
  10.6 76.2 all-gather.4
  154.8 15.1 all-gather.6
where the time goes:
time: 244 us; the launch traced here: 243 us
  Pallas kernels  108 us (44%)
  matrix products  38.1 us (16%)
  waiting for transfers between devices  31.8 us (13%)
  local copies, waits for them, and re-layouts  20.9 us (9%)
  starting transfers between devices  19.9 us (8%)
  between operations  15.1 us (6%)
  other arithmetic  9.3 us (4%)
    pallas_call x1, Pallas kernels, dispatched(): pl.pallas_call(functools.partial(dispatch_kernel, dims, cap), out_shape=j...  59.5 us
    pallas_call x1, Pallas kernels, returned(): pl.pallas_call(functools.partial(return_kernel, dims, cap), out_shape=jax...  48.1 us
    all_to_all x1, waiting for transfers between devices, sent_and_summed(): lax.all_to_all(blocks, axis, split_axis=0, concat_axis=0, tiled=True)  25.9 us
    all_to_all x1, starting transfers between devices, sent_and_summed(): lax.all_to_all(blocks, axis, split_axis=0, concat_axis=0, tiled=True)  12.7 us
    all_to_all x1, starting transfers between devices, copy_for_each(): return lax.all_to_all(copies, axis, split_axis=0, concat_axis=0, tiled=True)  7.16 us
    slice x24, local copies, waits for them, and re-layouts, joined_by_halves(): part[side::2]  7.12 us
    dot_general x1, matrix products, expert_backward(): jnp.einsum('rd,rf->df', inputs, gate_grad, preferred_element_type=jnp.flo...  5.91 us
    dot_general x1, matrix products, expert_backward(): jnp.einsum('rd,rf->df', inputs, up_grad, preferred_element_type=jnp.float32)  5.65 us
  transfers between devices with their start and end apart: 4, of which 3 were waited for; matrix products, arithmetic and copies ran while one was open for 22% of the time, Pallas kernels for 44%

commit v1 on v0

--- a/solution.py
+++ b/solution.py
@@ -181,16 +181,45 @@
 
 
 def return_kernel(
-    dims, cap, part, target, cot, out, pair, sums, far, near, back, mine, moe, own_sem,
-    p_send, p_recv, y_send, y_recv, r_send, r_recv, m_send, m_recv,
+    dims, cap, part, target, cot, rmap, xmem, hid, fade, extra, rtile, itile, both, acts3,
+    gate_out, up_out, down_out, proj_out, lru_out,
+    pair, sums, far, near, back, mine, moe, mixed, xy, acts, grads, wide, held, turned, cross,
+    fold, rest, levels, pieces, alphas, betas, weights, small,
+    own_sem, p_send, p_recv, y_send, y_recv, r_send, r_recv, m_send, m_recv, in_sem, out_sem,
+    b_send, b_recv, z_send, z_recv, s_send, s_recv, h_send, h_recv, t_send, t_recv, a_send, a_recv,
+    g_send, g_recv, q_send, q_recv,
 ):
     nz, nx, ny = dims
     z, x, c, y = place()
-    barrier, greetings = greet_peers(dims, True)
+    plane = nz * nx * 2
+    index = (z * nx + x) * 2 + c
     width = cot.shape[1] // ny
+    toks = cot.shape[0]
     half = nz * nx * cap
     mid = half // 2
-    pl.semaphore_wait(barrier, greetings)
+    barrier = pltpu.get_barrier_semaphore()
+
+    def sp_at(i):
+        i = lax.rem(index + i, plane)
+        return (i // (2 * nx), lax.rem(i // 2, nx), lax.rem(i, 2), y)
+
+    def greet(i, _):
+        pl.semaphore_signal(barrier, inc=1, device_id=sp_at(i), device_id_type=MESH)
+        return 0
+
+    lax.fori_loop(1, plane, greet, 0)
+    for step in (1, 2, 3):
+        to = (z, x, c, lax.rem(y + step, ny))
+        pl.semaphore_signal(barrier, inc=1, device_id=to, device_id_type=MESH)
+
+    loads = [pltpu.make_async_copy(both, xy, in_sem.at[0])]
+    for m in range(3):
+        loads.append(pltpu.make_async_copy(acts3[m], acts.at[m], in_sem.at[m + 1]))
+    for load in loads:
+        load.start()
+    wide[z, x, c] = rmap[...]
+    held[x, c] = hid[...]
+    pl.semaphore_wait(barrier, plane - 1 + 3)
 
     def cols(turn):
         return pl.ds(pl.multiple_of(lax.rem(y + turn, ny) * width, 128), width)
@@ -201,14 +230,74 @@
             device_id_type=MESH,
         ).start()
 
+    other = (z, x, 1 - c, y)
     theirs = pl.ds(pl.multiple_of((1 - c) * half, cap), half)
     ours = pl.multiple_of(c * half, cap)
-    order = (2, 1, 3, 0)
-    for turn in order:
+    for turn in (2, 1, 3, 0):
         remote(
-            part.at[theirs, cols(turn)], pair.at[turn], p_send.at[turn], p_recv.at[turn],
-            (z, x, 1 - c, y),
+            part.at[theirs, cols(turn)], pair.at[turn], p_send.at[turn], p_recv.at[turn], other
         )
+    for step in range(1, nx):
+        to = (z, lax.rem(x + step, nx), c, y)
+        remote(rmap, wide.at[z, x, c], b_send.at[step - 1], b_recv.at[step - 1], to)
+    for step in range(1, nx):
+        to = (z, lax.rem(x + step, nx), c, y)
+        remote(hid, held.at[x, c], h_send.at[step - 1], h_recv.at[step - 1], to)
+
+    chunk = 256
+
+    def weight_grad(m):
+        def some(i, _):
+            here = pl.ds(pl.multiple_of(i * chunk, chunk), chunk)
+            grads[m, :, here] = jnp.dot(
+                acts[m], xy[m // 2, :, here], preferred_element_type=F32
+            ).astype(BF16)
+            return 0
+
+        lax.fori_loop(0, cot.shape[1] // chunk, some, 0)
+        pltpu.make_async_copy(
+            grads.at[m], (gate_out, up_out, down_out)[m], out_sem.at[m]
+        ).start()
+
+    rounds = nz // 2
+
+    def ring_block(s, side):
+        away = nz - s if side == 0 else s
+        from_z = lax.rem(z + away, nz)
+        if s < rounds:
+            return wide.at[from_z, :, c]
+        return wide.at[from_z, pl.ds(side * (nx // 2), nx // 2), c]
+
+    def ring_sent(s, side):
+        away = nz - s if side == 0 else s
+        from_z = lax.rem(z + away, nz)
+        if s < rounds - 1:
+            return wide.at[from_z, :, c]
+        return wide.at[from_z, pl.ds(side * (nx // 2), nx // 2), c]
+
+    def ring(s):
+        if s == 0:
+            for step in range(1, nx):
+                drained(rmap, b_recv.at[step - 1])
+            remote(wide.at[z, :, c], wide.at[z, :, c], s_send, s_recv, other)
+        else:
+            for side in range(2):
+                drained(ring_block(s, side), z_recv.at[side, s - 1])
+                remote(ring_block(s, side), ring_block(s, side), s_send, s_recv, other)
+        if s < rounds:
+            for side in range(2):
+                to = (lax.rem(z + (1 if side == 0 else nz - 1), nz), x, c, y)
+                some = ring_sent(s, side)
+                remote(some, some, z_send.at[side, s], z_recv.at[side, s], to)
+
+    loads[0].wait()
+    loads[1].wait()
+    weight_grad(0)
+    ring(0)
+    for step in range(1, nx):
+        drained(hid, h_recv.at[step - 1])
+    remote(held.at[:, c], held.at[:, c], t_send, t_recv, other)
+
     up, down = (z, x, c, lax.rem(y + 1, ny)), (z, x, c, lax.rem(y + 3, ny))
     low, high = pl.ds(0, mid), pl.ds(mid, mid)
 
@@ -233,6 +322,54 @@
     remote(sums.at[3, low], near.at[1, low], y_send.at[3], y_recv.at[3], down)
     added(0)
 
+    blocks, span = rtile.shape[0], rtile.shape[1]
+    for b in range(blocks):
+        here = pl.ds(b * span, span)
+        some = xmem[:, here]
+        rec = jax.nn.sigmoid(jnp.dot(some, rtile[b], preferred_element_type=F32))
+        inp = jax.nn.sigmoid(jnp.dot(some, itile[b], preferred_element_type=F32))
+        speed = -8.0 * fade[:, here]
+        log_decay = rec * speed + extra[...]
+        decay = jnp.exp(log_decay)
+        spare = 1.0 - jnp.exp(2.0 * log_decay)
+        scale = jnp.sqrt(jnp.maximum(spare, 0.01))
+        gated = inp * some.astype(F32)
+        slope = jnp.where(spare > 0.01, -decay * decay / scale, 0.0)
+        level = hid[:, here].astype(F32) - scale * gated + slope * gated
+        pieces[0, :, here] = level * speed * rec * (1.0 - rec)
+        pieces[1, :, here] = scale * gated * (1.0 - inp)
+        pieces[2, :, here] = scale * inp
+        pieces[4, :, here] = decay
+    row = lax.broadcasted_iota(jnp.int32, (toks, 128), 0)
+    reach = [1 << s for s in range(toks.bit_length() - 1)]
+
+    def products(i, _):
+        here = pl.ds(pl.multiple_of(i * 128, 128), 128)
+        decay = pieces[4, :, here]
+        prod = jnp.where(row < toks - 1, pltpu.roll(decay, toks - 1, 0), 1.0)
+        for n, s in enumerate(reach):
+            inside = row < toks - s
+            levels[n, :, here] = jnp.where(inside, prod, 0.0)
+            prod = prod * jnp.where(inside, pltpu.roll(prod, toks - s, 0), 1.0)
+        pieces[3, :, here] = prod
+        small[0, pl.ds(i, 1), :] = decay[0:1] * prod[0:1]
+        return 0
+
+    for i in range(width // 128):
+        products(i, 0)
+    betas[index] = small[0]
+
+    def tell(src, dst, send, recv):
+        def one(i, _):
+            remote(src, dst.at[index], send, recv, sp_at(i))
+            return 0
+
+        lax.fori_loop(1, plane, one, 0)
+
+    tell(small.at[0], betas, a_send.at[0], a_recv.at[0])
+
+    ring(1)
+
     def joined(side, turn, first):
         drained(far.at[side], y_recv.at[side])
 
@@ -249,6 +386,21 @@
     remote(sums.at[1, low], near.at[0, low], y_send.at[4], y_recv.at[4], up)
     joined(1, 3, mid)
     remote(sums.at[3, high], near.at[1, high], y_send.at[5], y_recv.at[5], down)
+
+    ring(2)
+    loads[2].wait()
+    weight_grad(1)
+    for s in range(3, rounds + 1):
+        ring(s)
+
+    drained(betas.at[pl.ds(0, plane - 1)], a_recv.at[0])
+
+    def weigh(j, run):
+        later = j > index
+        weights[j] = jnp.where(later, run, 0.0)
+        return jnp.where(later, run * betas[j], 1.0)
+
+    lax.fori_loop(0, plane, weigh, jnp.ones((width // 128, 128), F32))
 
     me = z * nx + x
 
@@ -280,17 +432,16 @@
     finished(mid, 2, 5)
     lax.fori_loop(nz * nx // 2, nz * nx, give, 0)
     finished(0, 4, 3)
-    own = pltpu.make_async_copy(
-        mine.at[pl.ds(pl.multiple_of(x * cap, cap), cap), :],
-        back.at[pl.ds(pl.multiple_of(me * cap, cap), cap), :],
-        own_sem,
-    )
-    own.start()
+    back[pl.ds(pl.multiple_of(me * cap, cap), cap), :] = mine[
+        pl.ds(pl.multiple_of(x * cap, cap), cap), :
+    ]
     lax.fori_loop(1, nz * nx // 2, give, 0)
-    slot = lax.broadcasted_iota(jnp.int32, (cot.shape[0], half), 1)
+
+    loads[3].wait()
+    weight_grad(2)
+    slot = lax.broadcasted_iota(jnp.int32, (toks, half), 1)
     chosen = (slot == target[:, 0:1]) | (slot == target[:, 1:2])
     onehot = jnp.where(chosen, 1.0, 0.0).astype(BF16)
-    own.wait()
     drained(back.at[pl.ds(0, half - cap), :], r_recv)
     moe[:, cols(0)] = jnp.dot(onehot, back[...], preferred_element_type=F32).astype(BF16)
     for step in (1, 3, 2):
@@ -300,7 +451,70 @@
         )
     for step in (1, 3, 2):
         drained(moe.at[:, cols(ny - step)], m_recv.at[step - 1])
-    out[...] = (cot[...].astype(F32) + moe[...].astype(F32)).astype(BF16)
+    mixed[...] = (cot[...].astype(F32) + moe[...].astype(F32)).astype(BF16)
+
+    lines = rmap.shape[0]
+    turned[...] = jnp.transpose(mixed[...]).reshape(nz, 2 * nx, lines, toks)
+    spot = x * 2 + c
+    cross[:, :, pl.ds(pl.multiple_of(spot * toks, toks), toks)] = turned[:, spot]
+
+    for step in range(1, 2 * nx):
+        to = lax.rem(spot + step, 2 * nx)
+        remote(
+            turned.at[:, to],
+            cross.at[:, :, pl.ds(pl.multiple_of(spot * toks, toks), toks)],
+            g_send.at[step - 1], g_recv.at[step - 1],
+            (z, to // 2, lax.rem(to, 2), y),
+        )
+
+    drained(wide.at[:, :, 1 - c], s_recv)
+    state = jnp.dot(
+        mixed[...], wide[...].reshape(-1, width), preferred_element_type=F32
+    )
+    for n, s in enumerate(reach):
+        state = state + levels[n] * pltpu.roll(state, toks - s, 0)
+    first = pieces[4, 0:1, :] * state[0:1]
+    for i in range(width // 128):
+        small[1, pl.ds(i, 1), :] = first[:, i * 128 : (i + 1) * 128]
+    alphas[index] = small[1]
+    tell(small.at[1], alphas, a_send.at[1], a_recv.at[1])
+
+    drained(held.at[:, 1 - c], t_recv)
+    for step in range(1, 2 * nx):
+        drained(turned.at[:, 0], g_recv.at[step - 1])
+    total = jnp.dot(
+        cross[...].reshape(nz * lines, 2 * nx * toks),
+        held[...].reshape(2 * nx * toks, width),
+        preferred_element_type=F32,
+    )
+    fold[...] = total.astype(BF16).reshape(nz, lines, width)
+    rest[z] = fold[z]
+    for step in range(1, nz):
+        to = lax.rem(z + step, nz)
+        remote(fold.at[to], rest.at[z], q_send.at[step - 1], q_recv.at[step - 1], (to, x, c, y))
+
+    drained(alphas.at[pl.ds(0, plane - 1)], a_recv.at[1])
+    carried = jnp.sum(weights[...] * alphas[...], axis=0)
+    carried = jnp.concatenate([carried[i : i + 1] for i in range(width // 128)], axis=1)
+    state = state + pieces[3] * carried
+    grad_rec = (state * pieces[0]).astype(BF16)
+    grad_in = (state * pieces[1]).astype(BF16)
+    direct = state * pieces[2]
+    turn_dims = (((1,), (1,)), ((), ()))
+    for b in range(blocks):
+        here = slice(b * span, (b + 1) * span)
+        lru_out[:, here] = (
+            direct[:, here]
+            + lax.dot_general(grad_rec[:, here], rtile[b], turn_dims, preferred_element_type=F32)
+            + lax.dot_general(grad_in[:, here], itile[b], turn_dims, preferred_element_type=F32)
+        )
+
+    for step in range(1, nz):
+        drained(fold.at[0], q_recv.at[step - 1])
+    summed = rest[0].astype(F32)
+    for i in range(1, nz):
+        summed = summed + rest[i].astype(F32)
+    proj_out[...] = summed
 
     for turn in range(4):
         drained(pair.at[turn], p_send.at[turn])
@@ -309,18 +523,47 @@
     drained(back.at[pl.ds(0, half - cap), :], r_send)
     for step in (1, 2, 3):
         drained(moe.at[:, cols(0)], m_send.at[step - 1])
-
-
-def returned(dims, cap, part, target, cot):
+    for step in range(nx - 1):
+        drained(rmap, b_send.at[step])
+        drained(hid, h_send.at[step])
+    for s in range(rounds):
+        for side in range(2):
+            drained(ring_sent(s, side), z_send.at[side, s])
+    drained(wide.at[:, :, c], s_send)
+    drained(held.at[:, c], t_send)
+    for i in range(2):
+        drained(betas.at[pl.ds(0, plane - 1)], a_send.at[i])
+    for step in range(2 * nx - 1):
+        drained(turned.at[:, 0], g_send.at[step])
+    for step in range(nz - 1):
+        drained(fold.at[0], q_send.at[step])
+    for m in range(3):
+        pltpu.make_async_copy(
+            grads.at[m], (gate_out, up_out, down_out)[m], out_sem.at[m]
+        ).wait()
+
+
+def return_entry(dims, cap, *refs):
+    return_kernel(dims, cap, *refs[:11], refs[11:14], *refs[14:])
+
+
+def returned(dims, cap, part, target, cot, rmap, xmem, hid, fade, extra, rtile, itile, both, acts):
     nz, nx, ny = dims
     half, width = nz * nx * cap, cot.shape[1] // ny
-    vmem = pl.BlockSpec(memory_space=pltpu.VMEM)
+    toks, feats = cot.shape
+    lines, units = rmap.shape[0], acts[0].shape[0]
+    plane, lanes, steps = nz * nx * 2, width // 128, toks.bit_length() - 1
+    vmem, anyw = pl.BlockSpec(memory_space=pltpu.VMEM), pl.BlockSpec(memory_space=pl.ANY)
     dma = pltpu.SemaphoreType.DMA
     return pl.pallas_call(
-        functools.partial(return_kernel, dims, cap),
-        out_shape=jax.ShapeDtypeStruct(cot.shape, BF16),
-        in_specs=[vmem] * 3,
-        out_specs=vmem,
+        functools.partial(return_entry, dims, cap),
+        out_shape=[jax.ShapeDtypeStruct((units, feats), BF16)] * 3
+        + [
+            jax.ShapeDtypeStruct((lines, width), F32),
+            jax.ShapeDtypeStruct((toks, width), F32),
+        ],
+        in_specs=[vmem] * 10 + [anyw] * 4,
+        out_specs=[anyw] * 3 + [vmem] * 2,
         scratch_shapes=[
             pltpu.VMEM((4, half, width), BF16),
             pltpu.VMEM((4, half, width), BF16),
@@ -328,100 +571,38 @@
             pltpu.VMEM((2, half, width), BF16),
             pltpu.VMEM((half, width), BF16),
             pltpu.VMEM((half, width), BF16),
-            pltpu.VMEM(cot.shape, BF16),
+            pltpu.VMEM((toks, feats), BF16),
+            pltpu.VMEM((toks, feats), BF16),
+            pltpu.VMEM(both.shape, BF16),
+            pltpu.VMEM((3,) + acts[0].shape, BF16),
+            pltpu.VMEM((3, units, feats), BF16),
+            pltpu.VMEM((nz, nx, 2, lines, width), BF16),
+            pltpu.VMEM((nx, 2, toks, width), BF16),
+            pltpu.VMEM((nz, 2 * nx, lines, toks), BF16),
+            pltpu.VMEM((nz, lines, 2 * nx * toks), BF16),
+            pltpu.VMEM((nz, lines, width), BF16),
+            pltpu.VMEM((nz, lines, width), BF16),
+            pltpu.VMEM((steps, toks, width), F32),
+            pltpu.VMEM((5, toks, width), F32),
+            pltpu.VMEM((plane, lanes, 128), F32),
+            pltpu.VMEM((plane, lanes, 128), F32),
+            pltpu.VMEM((plane, lanes, 128), F32),
+            pltpu.VMEM((2, lanes, 128), F32),
             dma, dma((4,)), dma((4,)), dma((6,)), dma((6,)), dma, dma, dma((3,)), dma((3,)),
+            dma((4,)), dma((3,)), dma((nx - 1,)), dma((nx - 1,)), dma((2, nz // 2)),
+            dma((2, nz // 2)), dma, dma, dma((nx - 1,)), dma((nx - 1,)), dma, dma, dma((2,)),
+            dma((2,)), dma((2 * nx - 1,)), dma((2 * nx - 1,)), dma((nz - 1,)), dma((nz - 1,)),
         ],
-        compiler_params=pltpu.CompilerParams(collective_id=1, has_side_effects=True),
+        compiler_params=pltpu.CompilerParams(
+            collective_id=1, has_side_effects=True, vmem_limit_bytes=60 * 2**20
+        ),
         name="give_back",
-    )(part, target, cot)
-
-
-def joined_along(blocks, dim):
-    dims = list(blocks.shape[1:])
-    dims[dim] *= blocks.shape[0]
-    return jnp.moveaxis(blocks, 0, dim).reshape(dims)
-
-
-def copy_for_each(shard, axis):
-    copies = jnp.broadcast_to(shard, (lax.axis_size(axis), *shard.shape))
-    return lax.all_to_all(copies, axis, split_axis=0, concat_axis=0, tiled=True)
-
-
-def stacked_from(shard, axes, turns):
-    blocks = shard
-    for k in turns:
-        blocks = lax.all_gather(blocks, axes[k])
-    done = turns[::-1]
-    back = [done.index(k) for k in range(len(axes))]
-    blocks = blocks.transpose(*back, *range(len(axes), blocks.ndim))
-    return blocks.reshape(-1, *shard.shape)
-
-
-def gather_axes(shard, axes, turns, dim):
-    return joined_along(stacked_from(shard, axes, turns), dim)
-
-
-def gathered_once(shard, axis):
-    leaves = jax.tree.leaves(shard)
-    turns = sorted(range(len(leaves)), key=lambda k: -leaves[k].size)
-    width = (1, *leaves[turns[0]].shape)[-1]
-    lines = [
-        jnp.pad(leaves[k].reshape(-1), (0, -leaves[k].size % width)).reshape(-1, width)
-        for k in turns
-    ]
-    both, at, found = (copy_for_each(jnp.concatenate(lines), axis), 0, {})
-    for k, line in zip(turns, lines):
-        slab = both[:, at : at + len(line)].reshape(len(both), -1)
-        found[k] = slab[:, : leaves[k].size].reshape(-1, *leaves[k].shape)
-        at += len(line)
-    numbers = iter(range(len(leaves)))
-    return jax.tree.map(lambda _: found[next(numbers)], shard)
-
-
-def joined_by_halves(pieces, combine):
-    while len(jax.tree.leaves(pieces)[0]) > 1:
-        pieces = jax.vmap(combine)(
-            *(jax.tree.map(lambda part: part[side::2], pieces) for side in (0, 1))
-        )
-    return jax.tree.map(lambda part: part[0], pieces)
-
-
-def entering(shard, axis, combine, identity):
-    length, mine = (lax.axis_size(axis), lax.axis_index(axis))
-    passed = jnp.arange(length) > mine
-
-    def kept(part, zero, own):
-        part = jnp.where(
-            passed.reshape(-1, *(1 for _ in own.shape)), part, jnp.asarray(zero, own.dtype)
-        )
-        return part[::-1]
-
-    pieces = gathered_once(shard, axis)
-    return joined_by_halves(jax.tree.map(kept, pieces, identity, shard), combine)
-
-
-def in_blocks(shard, dim, length):
-    before, after = (shard.shape[:dim], shard.shape[dim + 1 :])
-    return jnp.moveaxis(shard.reshape(*before, length, -1, *after), dim, 0)
-
-
-def sent_and_summed(shard, axis, dim):
-    blocks = in_blocks(shard, dim, lax.axis_size(axis))
-    arrived = lax.all_to_all(blocks, axis, split_axis=0, concat_axis=0, tiled=True)
-    return arrived.astype(jnp.float32).sum(axis=0)
+    )(part, target, cot, rmap, xmem, hid, fade, extra, rtile, itile, both, *acts)
 
 
 def silu_slope(value):
     sig_value = jax.nn.sigmoid(value)
     return sig_value * (1.0 + value * (1.0 - sig_value))
-
-
-def compose(upper_map, lower_map):
-    return (lower_map[0] * upper_map[0], lower_map[1] + lower_map[0] * upper_map[1])
-
-
-def chain_join(higher_map, lower_map):
-    return (lower_map[0] * higher_map[0], lower_map[1] + lower_map[0] * higher_map[1])
 
 
 def expert_backward(inputs, grads_in, gate_weight, up_weight, down_weight):
@@ -429,23 +610,14 @@
     up_value = jnp.dot(inputs, up_weight, preferred_element_type=jnp.float32)
     active = jax.nn.silu(gate_value)
     hidden = (active * up_value).astype(jnp.bfloat16)
-    down_grad = jnp.einsum(
-        "rf,rd->fd", hidden, grads_in, preferred_element_type=jnp.float32
-    ).astype(jnp.bfloat16)
     hidden_grad = jnp.einsum("rd,fd->rf", grads_in, down_weight, preferred_element_type=jnp.float32)
     gate_grad = (hidden_grad * up_value * silu_slope(gate_value)).astype(jnp.bfloat16)
     up_grad = (hidden_grad * active).astype(jnp.bfloat16)
-    gate_weight_grad = jnp.einsum(
-        "rd,rf->df", inputs, gate_grad, preferred_element_type=jnp.float32
-    ).astype(jnp.bfloat16)
-    up_weight_grad = jnp.einsum(
-        "rd,rf->df", inputs, up_grad, preferred_element_type=jnp.float32
-    ).astype(jnp.bfloat16)
     token_part = jnp.einsum("rf,df->rd", gate_grad, gate_weight, preferred_element_type=jnp.float32)
     token_part = token_part + jnp.einsum(
         "rf,df->rd", up_grad, up_weight, preferred_element_type=jnp.float32
     )
-    return (gate_weight_grad, up_weight_grad, down_grad, token_part)
+    return gate_grad.T, up_grad.T, hidden.T, token_part.astype(jnp.bfloat16)
 
 
 def local(
@@ -482,99 +654,32 @@
         result_cotangent_values,
         specialist_entry_vectors,
     )
-    gate_weight_grad, up_weight_grad, down_grad, token_part = expert_backward(
+    *acts, token_part = expert_backward(
         both[0],
         both[1],
         specialist_switch_maps[0],
         specialist_widen_maps[0],
         specialist_shrink_maps[0],
     )
-    mixed_grad = returned(
+    gate_weight_grad, up_weight_grad, down_grad, out_proj_grad, lru_input_grad = returned(
         dims,
         capacity,
-        token_part.astype(jnp.bfloat16),
+        token_part,
         target.reshape(route_count, tok_rows).T,
         result_cotangent_values,
-    )
-    col_count = memory_readout_map.shape[1]
-    columns = mixed_grad
-    upstream = jnp.dot(
-        columns,
-        gather_axes(memory_readout_map, (("sp_0", "sp_1"), "sp_2"), (0, 1), 0),
-        preferred_element_type=jnp.float32,
-    )
-    blocks_here = memory_switch_tiles.shape[0]
-    block_width = memory_switch_tiles.shape[1]
-    blocks_in = memory_source_vectors.reshape(tok_rows, blocks_here, block_width)
-    memory_switch_fraction = jax.nn.sigmoid(
-        jnp.einsum(
-            "tnc,ncd->tnd", blocks_in, memory_switch_tiles, preferred_element_type=jnp.float32
-        ).reshape(tok_rows, col_count)
-    )
-    inp_open = jax.nn.sigmoid(
-        jnp.einsum(
-            "tnc,ncd->tnd", blocks_in, entry_switch_tiles, preferred_element_type=jnp.float32
-        ).reshape(tok_rows, col_count)
-    )
-    xin = memory_source_vectors.astype(jnp.float32)
-    log_fading_factor = (
-        -8.0 * memory_switch_fraction * feature_fading_speed[None, :] + extra_log_fading[:, None]
-    )
-    decay_mult = jnp.exp(log_fading_factor)
-    spare_room = -jnp.expm1(2.0 * log_fading_factor)
-    in_scale = jnp.sqrt(jnp.maximum(spare_room, 0.01))
-    drive = in_scale * inp_open * xin
-    coeff = jnp.concatenate([decay_mult[1:], jnp.ones((1, col_count), jnp.float32)], axis=0)
-    prod_after, local_part = lax.associative_scan(compose, (coeff, upstream), reverse=True, axis=0)
-    alpha_part = decay_mult[0] * local_part[0]
-    beta_part = decay_mult[0] * prod_after[0]
-    carried = entering(
-        (beta_part, alpha_part),
-        SP,
-        chain_join,
-        (jnp.ones_like(beta_part), jnp.zeros_like(alpha_part)),
-    )
-    incoming = carried[1]
-    dstate = local_part + prod_after * incoming[None, :]
-    scale_slope = jnp.where(spare_room > 0.01, -decay_mult * decay_mult / in_scale, 0.0)
-    log_grad = dstate * (
-        memory_hidden_values.astype(jnp.float32) - drive + scale_slope * inp_open * xin
-    )
-    grad_rec = (
-        log_grad
-        * (-8.0 * feature_fading_speed[None, :])
-        * memory_switch_fraction
-        * (1.0 - memory_switch_fraction)
-    ).astype(jnp.bfloat16)
-    grad_in = (dstate * in_scale * xin * inp_open * (1.0 - inp_open)).astype(jnp.bfloat16)
-    back_rec = jnp.einsum(
-        "tnd,ncd->tnc",
-        grad_rec.reshape(tok_rows, blocks_here, block_width),
+        memory_readout_map,
+        memory_source_vectors,
+        memory_hidden_values,
+        feature_fading_speed[None, :],
+        extra_log_fading[:, None],
         memory_switch_tiles,
-        preferred_element_type=jnp.float32,
-    )
-    back_in = jnp.einsum(
-        "tnd,ncd->tnc",
-        grad_in.reshape(tok_rows, blocks_here, block_width),
         entry_switch_tiles,
-        preferred_element_type=jnp.float32,
-    )
-    lru_input_grad = (
-        dstate * in_scale * inp_open
-        + back_rec.reshape(tok_rows, col_count)
-        + back_in.reshape(tok_rows, col_count)
-    )
-    columns = mixed_grad
-    out_proj_grad = sent_and_summed(
-        jnp.einsum(
-            "tr,tc->rc", columns, memory_hidden_values, preferred_element_type=jnp.float32
-        ).astype(jnp.bfloat16),
-        SP,
-        0,
+        both,
+        acts,
     )
     return (
-        gate_weight_grad[None],
-        up_weight_grad[None],
+        gate_weight_grad.T[None],
+        up_weight_grad.T[None],
         down_grad[None],
         out_proj_grad,
         lru_input_grad,

time: 244 us -> 170 us (0.70)
  waiting for transfers between devices: 31.8 us -> 0 us
  Pallas kernels: 108 us -> 137 us
  starting transfers between devices: 19.9 us -> 0 us
  matrix products: 38.1 us -> 18.9 us
  between operations: 15.1 us -> 0.73 us
  local copies, waits for them, and re-layouts: 20.9 us -> 11.8 us
  other arithmetic: 9.3 us -> 1.41 us
    all_to_all x2 -> x0, waiting for transfers between devices: 30.6 us -> none  [the longest x1 25.9 us: sent_and_summed(): lax.all_to_all(blocks, axis, split_axis=0, concat_axis=0, tiled=True)]
    pallas_call x1, Pallas kernels: 48.1 us -> 77.5 us  [returned(): pl.pallas_call(functools.partial(return_entry, dims, cap), out_shape=[jax...]
    dot_general x9 -> x0, matrix products: 22.2 us -> none  [the longest x1 5.91 us: expert_backward(): jnp.einsum('rd,rf->df', inputs, gate_grad, preferred_element_type=jnp.flo...]
    all_to_all x2 -> x0, starting transfers between devices: 19.8 us -> none  [the longest x1 12.7 us: sent_and_summed(): lax.all_to_all(blocks, axis, split_axis=0, concat_axis=0, tiled=True)]
    slice x75 -> x0, local copies, waits for them, and re-layouts: 10.4 us -> none  [the longest x24 7.12 us: joined_by_halves(): part[side::2]]
    unnamed x48 -> x25, local copies, waits for them, and re-layouts: 3.98 us -> 10.8 us
    reduce_sum x1 -> x0, other arithmetic: 2.54 us -> none  [sent_and_summed(): return arrived.astype(jnp.float32).sum(axis=0)]
  transfers between devices with their start and end apart: 4 -> 0, of which waited for: 3 -> 0; matrix products, arithmetic and copies ran while one was open for 22% -> 0% of each run, Pallas kernels for 44% -> 0%
where the time goes in v1:
time: 170 us
  Pallas kernels  137 us (81%)
  matrix products  18.9 us (11%)
  local copies, waits for them, and re-layouts  11.8 us (7%)
    pallas_call x1, Pallas kernels, returned(): pl.pallas_call(functools.partial(return_entry, dims, cap), out_shape=[jax...  77.5 us
    pallas_call x1, Pallas kernels, dispatched(): pl.pallas_call(functools.partial(dispatch_kernel, dims, cap), out_shape=j...  59.5 us
    unnamed x25, local copies, waits for them, and re-layouts  10.8 us
    dot_general x1, matrix products, expert_backward(): jnp.dot(inputs, gate_weight, preferred_element_type=jnp.float32)  5 us
    dot_general x1, matrix products, expert_backward(): jnp.einsum('rf,df->rd', up_grad, up_weight, preferred_element_type=jnp.fl...  4.68 us
    dot_general x1, matrix products, expert_backward(): up_value = jnp.dot(inputs, up_weight, preferred_element_type=jnp.float32)  4.31 us

profile of v1, /device:TPU:1, one launch (start us, length us, event | category | flops | bytes accessed | tf_op | source)
XLA Modules:
  0.0 169.9 jit_solution(6551811633187009246)
XLA Ops:
  0.6 0.0 copy-start
  0.6 0.9 copy.34
  1.6 0.1 copy.37
  1.6 0.2 convert_reduce_fusion
  1.8 0.1 copy.39
  1.9 0.6 add_bitcast_fusion
  2.6 0.1 copy.36
  2.6 0.6 add.60.target
  3.2 1.4 copy.38.share
  4.6 59.5 %dispatch.1.refs_10_ = bf16[2,1024,2048]{2,1,0:T(8,128)(2,1)} custom-call(s32[1,256]{1,0:T(1,128)} %add.60.target, f32[128,2]{1,0:T(8,128)} %copy.38.share, bf16[128,2048]{1,0:T(8,128)(2,1)} %refs_2_.1, bf16[128,2048]{1,0:T(8,128)(2,1)} %rows.1), custom_call_target="tpu_custom_call" | custom-call | tf_op jit(solution)/shard_map/dispatch/pallas_call | solution.py:169
  64.2 0.0 copy-start.1
  64.2 0.0 copy-start.7
  64.2 5.0 %fusion = f32[1024,448]{0,1:T(8,128)S(1)} fusion(bf16[2,1024,2048]{2,1,0:T(8,128)(2,1)} %dispatch.1.refs_10_, bf16[1,2048,448]{1,2,0:T(8,128)(2,1)} %param.18), kind=kOutput, calls=%fused_computation.1 | convolution fusion | flops 1879048192 | bytes 7864320 | tf_op jit(solution)/shard_map/dot_general | solution.py:609
  69.2 0.1 copy-done.1
  69.3 0.5 copy-done.7
  69.8 2.1 %fusion.4 = f32[1024,448]{0,1:T(8,128)S(1)} fusion(bf16[2,1024,2048]{2,1,0:T(8,128)(2,1)S(1)} %copy-done.1, bf16[1,448,2048]{2,1,0:T(8,128)(2,1)S(1)} %copy-done.7), kind=kOutput, calls=%fused_computation.5 | convolution fusion | flops 1879048192 | bytes 7864320 | tf_op jit(solution)/shard_map/rd,fd->rf/dot_general | solution.py:613
  71.9 0.0 copy-done
  72.0 0.0 copy-start.8
  72.0 4.3 %fusion.16 = (bf16[448,1024]{1,0:T(8,128)(2,1)}, bf16[448,1024]{1,0:T(8,128)(2,1)}, bf16[448,1024]{1,0:T(8,128)(2,1)}, f32[1024,448]{0,1:T(8,128)S(1)}) fusion(f32[1024,448]{0,1:T(8,128)S(1)} %fusion, f32[1024,448]{0,1:T(8,128)S(1)} %fusion.4, bf16[1,2048,448]{1,2,0:T(8,128)(2,1)S(1)} %copy-done, bf16[2,1024,2048]{2,1,0:T(8,128)(2,1)S(1)} %copy-done.1), kind=kOutput, calls=%fused_computation.22 | convolution fusion | flops 1885929472 | bytes 14286848 | tf_op jit(solution)/shard_map/dot_general | solution.py:610
  76.3 0.0 copy-done.8
  76.3 2.8 %fusion.18 = f32[1024,2048]{1,0:T(8,128)S(1)} fusion(bf16[1,2048,448]{1,2,0:T(8,128)(2,1)S(1)} %copy-done.8, f32[1024,448]{0,1:T(8,128)S(1)} %fusion, f32[1024,448]{0,1:T(8,128)S(1)} %fusion.4, f32[1024,448]{0,1:T(8,128)S(1)} %get-tuple-element.20), kind=kOutput, calls=%fused_computation.25 | convolution fusion | flops 1883635712 | bytes 15728640 | tf_op jit(solution)/shard_map/rf,df->rd/dot_general | solution.py:616
  79.0 0.0 copy-start.6
  79.1 4.7 %add_convert_fusion.refs_0_ = bf16[1024,2048]{1,0:T(8,128)(2,1)} fusion(f32[1024,2048]{1,0:T(8,128)S(1)} %fusion.18, bf16[1,2048,448]{1,2,0:T(8,128)(2,1)S(1)} %copy-done, f32[1024,448]{0,1:T(8,128)S(1)} %fusion.4, f32[1024,448]{0,1:T(8,128)S(1)} %fusion), kind=kOutput, calls=%fused_computation | convolution fusion | flops 1885995008 | bytes 18087936 | tf_op jit(solution)/shard_map/rf,df->rd/dot_general | solution.py:617
  83.7 0.0 copy-done.6
  83.7 0.7 copy.40.refs_7_
  84.5 77.5 %give_back.1 = (bf16[448,2048]{1,0:T(8,128)(2,1)}, bf16[448,2048]{1,0:T(8,128)(2,1)}, bf16[448,2048]{1,0:T(8,128)(2,1)}, f32[32,512]{1,0:T(8,128)}, f32[128,512]{1,0:T(8,128)}) custom-call(bf16[1024,2048]{1,0:T(8,128)(2,1)} %add_convert_fusion.refs_0_, s32[128,2]{1,0:T(8,128)} %get-tuple-element.18.refs_1_, bf16[128,2048]{1,0:T(8,128)(2,1)} %refs_2_.1, ...), custom_call_target="tpu_custom_call" | custom-call | tf_op jit(solution)/shard_map/give_back/pallas_call | solution.py:558
  162.0 0.0 copy-start.3
  162.0 3.1 %copy.46 = bf16[1,2048,448]{1,2,0:T(8,128)(2,1)} copy(bf16[1,2048,448]{1,2,0:T(8,128)(2,1)} %bitcast.86) | data formatting | bytes 3670016
  165.1 0.0 copy-done.3
  165.1 0.0 copy-start.2
  165.1 1.2 copy.47
  166.3 0.9 copy-done.2
  167.3 0.0 copy-start.5
  167.3 0.0 copy-start.4
  167.3 1.2 copy.48
  168.5 0.0 copy-done.5
  168.5 0.6 copy.49
  169.1 0.0 copy-done.4
  169.1 0.7 copy.50
  (2 shorter events, 0.0 us)
Async XLA Ops:
  0.6 71.3 %copy-start = (bf16[1,2048,448]{1,2,0:T(8,128)(2,1)S(1)}, bf16[1,2048,448]{1,2,0:T(8,128)(2,1)}, u32[]{:S(2)}) copy-start(bf16[1,2048,448]{1,2,0:T(8,128)(2,1)} %param.19) | copy-start | bytes 5505028
  64.2 5.2 %copy-start.1 = (bf16[2,1024,2048]{2,1,0:T(8,128)(2,1)S(1)}, bf16[2,1024,2048]{2,1,0:T(8,128)(2,1)}, u32[]{:S(2)}) copy-start(bf16[2,1024,2048]{2,1,0:T(8,128)(2,1)} %dispatch.1.refs_10_) | copy-start | bytes 25165828
  64.2 5.7 %copy-start.7 = (bf16[1,448,2048]{2,1,0:T(8,128)(2,1)S(1)}, bf16[1,448,2048]{2,1,0:T(8,128)(2,1)}, u32[]{:S(2)}) copy-start(bf16[1,448,2048]{2,1,0:T(8,128)(2,1)} %param.20) | copy-start | bytes 5505028
  72.0 4.3 %copy-start.8 = (bf16[1,2048,448]{1,2,0:T(8,128)(2,1)S(1)}, bf16[1,2048,448]{1,2,0:T(8,128)(2,1)}, u32[]{:S(2)}) copy-start(bf16[1,2048,448]{1,2,0:T(8,128)(2,1)} %param.18) | copy-start | bytes 5505028
  79.0 4.7 %copy-start.6 = (f32[128]{0:T(128)S(1)}, f32[128]{0:T(128)}, u32[]{:S(2)}) copy-start(f32[128]{0:T(128)} %param.25) | copy-start | bytes 1540
  162.0 3.1 %copy-start.3 = (bf16[448,2048]{1,0:T(8,128)(2,1)S(1)}, bf16[448,2048]{1,0:T(8,128)(2,1)}, u32[]{:S(2)}) copy-start(bf16[448,2048]{1,0:T(8,128)(2,1)} %get-tuple-element.11) | copy-start | bytes 5505028
  165.1 2.2 %copy-start.2 = (bf16[448,2048]{1,0:T(8,128)(2,1)S(1)}, bf16[448,2048]{1,0:T(8,128)(2,1)}, u32[]{:S(2)}) copy-start(bf16[448,2048]{1,0:T(8,128)(2,1)} %get-tuple-element.12) | copy-start | bytes 5505028
  167.3 1.2 copy-start.5
  167.3 1.9 %copy-start.4 = (f32[128,512]{1,0:T(8,128)S(1)}, f32[128,512]{1,0:T(8,128)}, u32[]{:S(2)}) copy-start(f32[128,512]{1,0:T(8,128)} %get-tuple-element.30) | copy-start | bytes 786436

commit v2 on v1

v2 whole, which is shorter than its diff:
```python
import functools

import jax
import jax.numpy as jnp
from jax import lax
from jax.experimental import pallas as pl
from jax.experimental.pallas import tpu as pltpu
from jax.sharding import Mesh
from jax.sharding import PartitionSpec as P

SLICES = 2
SP = ("sp_0", "sp_1", "sp_2")
MESH = pl.DeviceIdType.MESH
F32, BF16 = jnp.float32, jnp.bfloat16


def place():
    return tuple(lax.axis_index(n) for n in ("sp_0", "sp_1", "sp_2", "tp"))


def offset_of(k, count):
    odd = lax.rem(k, 2)
    return lax.rem(odd * ((k + 1) // 2) + (1 - odd) * (count - k // 2), count)


def drained(ref, sem):
    pltpu.make_async_copy(ref, ref, sem).wait()


def layer_kernel(
    dims, cap, target, spots, share, cot, rows, rmap, xmem, hid, fade, extra, rtile, itile, maps,
    outs, proj_out, lru_out,
    slots, xy, wts, accs, acts, give_rows, own_rows, pair, sums, far, near, back, mine, moe, mixed,
    grads, wide, held, turned, cross, fold, rest, levels, pieces, alphas, betas, weights, small,
    own_sem, in_sem, out_sem, d_send, d_recv, y_send, y_recv, f_send, f_recv, c_send, c_recv,
    p_send, p_recv, e_send, e_recv, r_send, r_recv, m_send, m_recv, b_send, b_recv, z_send, z_recv,
    s_send, s_recv, h_send, h_recv, t_send, t_recv, a_send, a_recv, g_send, g_recv, q_send, q_recv,
):
    nz, nx, ny = dims
    z, x, c, y = place()
    plane = nz * nx * 2
    index = (z * nx + x) * 2 + c
    me = z * nx + x
    toks, feats = cot.shape
    width = feats // ny
    half = nz * nx * cap
    group = nx * cap
    other = (z, x, 1 - c, y)
    up, down = (z, x, c, lax.rem(y + 1, ny)), (z, x, c, lax.rem(y + 3, ny))
    barrier = pltpu.get_barrier_semaphore()

    def sp_at(i):
        i = lax.rem(index + i, plane)
        return (i // (2 * nx), lax.rem(i // 2, nx), lax.rem(i, 2), y)

    def greet(i, _):
        pl.semaphore_signal(barrier, inc=1, device_id=sp_at(i), device_id_type=MESH)
        return 0

    lax.fori_loop(1, plane, greet, 0)
    for step in (1, 2, 3):
        to = (z, x, c, lax.rem(y + step, ny))
        pl.semaphore_signal(barrier, inc=1, device_id=to, device_id_type=MESH)

    def cols(turn):
        return pl.ds(pl.multiple_of(lax.rem(y + turn, ny) * width, 128), width)

    def remote(src, dst, send, recv, to):
        pltpu.make_async_remote_copy(
            src_ref=src, dst_ref=dst, send_sem=send, recv_sem=recv, device_id=to,
            device_id_type=MESH,
        ).start()

    loads = [pltpu.make_async_copy(maps[m], wts.at[m], in_sem.at[m]) for m in range(3)]
    for load in loads:
        load.start()
    wide[z, x, c] = rmap[...]
    held[x, c] = hid[...]

    slot = lax.broadcasted_iota(jnp.int32, (half, target.shape[1]), 0)
    onehot = jnp.where(slot == target[...], 1.0, 0.0).astype(BF16)
    some = rows[:, cols(0)]
    slots[0] = jnp.dot(
        onehot, jnp.concatenate([some, some], axis=0), preferred_element_type=F32
    ).astype(BF16)
    some = cot[:, cols(0)].astype(F32)
    scaled = [(share[:, k : k + 1] * some).astype(BF16) for k in range(2)]
    slots[1] = jnp.dot(
        onehot, jnp.concatenate(scaled, axis=0), preferred_element_type=F32
    ).astype(BF16)

    def source(e):
        return slots.at[:, pl.ds(pl.multiple_of(e * cap, cap), cap), :]

    def landing(k):
        start = pl.multiple_of(c * half + (k * nx + x) * cap, cap)
        return xy.at[:, pl.ds(start, cap), cols(0)]

    here = pl.ds(pl.multiple_of(c * half + x * cap, cap), cap)
    mine_too = pl.ds(pl.multiple_of(me * cap, cap), cap)
    for i in range(2):
        xy[i, here, cols(0)] = slots[i, mine_too, :]
    pl.semaphore_wait(barrier, plane - 1 + 3)

    def push(i, _):
        k, dx = i // nx, lax.rem(i, nx)
        tz, tx = lax.rem(z + offset_of(k, nz), nz), lax.rem(x + dx, nx)
        remote(source(tz * nx + tx), landing(k), d_send, d_recv.at[k], (tz, tx, c, y))
        return 0

    lax.fori_loop(1, nz * nx, push, 0)
    for step in range(1, nx):
        to = (z, lax.rem(x + step, nx), c, y)
        remote(rmap, wide.at[z, x, c], b_send.at[step - 1], b_recv.at[step - 1], to)
        remote(hid, held.at[x, c], h_send.at[step - 1], h_recv.at[step - 1], to)

    rounds = nz // 2

    def ring_block(s, side, halved):
        away = nz - s if side == 0 else s
        from_z = lax.rem(z + away, nz)
        if halved:
            return wide.at[from_z, pl.ds(side * (nx // 2), nx // 2), c]
        return wide.at[from_z, :, c]

    def ring_sent(s, side):
        return ring_block(s, side, s == rounds - 1)

    def ring(s):
        if s == 0:
            for step in range(1, nx):
                drained(rmap, b_recv.at[step - 1])
            remote(wide.at[z, :, c], wide.at[z, :, c], s_send, s_recv, other)
        else:
            for side in range(2):
                some = ring_block(s, side, s == rounds)
                drained(some, z_recv.at[side, s - 1])
                remote(some, some, s_send, s_recv, other)
        if s < rounds:
            for side in range(2):
                to = (lax.rem(z + (1 if side == 0 else nz - 1), nz), x, c, y)
                some = ring_sent(s, side)
                remote(some, some, z_send.at[side, s], z_recv.at[side, s], to)

    blocks, span = rtile.shape[0], rtile.shape[1]
    row = lax.broadcasted_iota(jnp.int32, (toks, 128), 0)
    reach = [1 << s for s in range(toks.bit_length() - 1)]

    def gates():
        for b in range(blocks):
            here = pl.ds(b * span, span)
            some = xmem[:, here]
            rec = jax.nn.sigmoid(jnp.dot(some, rtile[b], preferred_element_type=F32))
            inp = jax.nn.sigmoid(jnp.dot(some, itile[b], preferred_element_type=F32))
            speed = -8.0 * fade[:, here]
            log_decay = rec * speed + extra[...]
            decay = jnp.exp(log_decay)
            spare = 1.0 - jnp.exp(2.0 * log_decay)
            scale = jnp.sqrt(jnp.maximum(spare, 0.01))
            gated = inp * some.astype(F32)
            slope = jnp.where(spare > 0.01, -decay * decay / scale, 0.0)
            level = hid[:, here].astype(F32) - scale * gated + slope * gated
            pieces[0, :, here] = level * speed * rec * (1.0 - rec)
            pieces[1, :, here] = scale * gated * (1.0 - inp)
            pieces[2, :, here] = scale * inp
            pieces[4, :, here] = decay

    def tell(src, dst, send, recv):
        def one(i, _):
            remote(src, dst.at[index], send, recv, sp_at(i))
            return 0

        lax.fori_loop(1, plane, one, 0)

    def products():
        for i in range(width // 128):
            here = pl.ds(i * 128, 128)
            decay = pieces[4, :, here]
            prod = jnp.where(row < toks - 1, pltpu.roll(decay, toks - 1, 0), 1.0)
            for n, s in enumerate(reach):
                inside = row < toks - s
                levels[n, :, here] = jnp.where(inside, prod, 0.0)
                prod = prod * jnp.where(inside, pltpu.roll(prod, toks - s, 0), 1.0)
            pieces[3, :, here] = prod
            small[0, pl.ds(i, 1), :] = decay[0:1] * prod[0:1]
        betas[index] = small[0]
        tell(small.at[0], betas, a_send.at[0], a_recv.at[0])

    def weigh_all():
        drained(betas.at[pl.ds(0, plane - 1)], a_recv.at[0])

        def weigh(j, run):
            later = j > index
            weights[j] = jnp.where(later, run, 0.0)
            return jnp.where(later, run * betas[j], 1.0)

        lax.fori_loop(0, plane, weigh, jnp.ones((width // 128, 128), F32))

    def block(k, turn):
        start = pl.multiple_of(c * half + k * group, cap)
        return xy.at[:, pl.ds(start, group), cols(turn)]

    def across(k, turn):
        remote(block(k, turn), block(k, turn), c_send, c_recv, other)

    def along(k, turn, to, send, recv):
        remote(block(k, turn), block(k, turn), send, recv, to)

    turn_dims = (((1,), (1,)), ((), ()))
    piece = min(256, half)

    def forward(side, turn, first):
        def some(i, _):
            m, n = i // (half // piece), lax.rem(i, half // piece)
            here = pl.ds(pl.multiple_of(side * half + n * piece, cap), piece)
            got = lax.dot_general(
                wts[m, :, cols(turn)], xy[m // 2, here, cols(turn)], turn_dims,
                preferred_element_type=F32,
            )
            if first:
                accs[m, :, here] = got
            else:
                accs[m, :, here] += got
            return 0

        lax.fori_loop(0, 3 * (half // piece), some, 0)

    for turn in range(nz + 3):
        k = turn
        if k < nz:
            if k == 0:
                drained(slots.at[:, pl.ds(0, group - cap), :], d_recv.at[0])
            else:
                drained(block(k, 0), d_recv.at[k])
            along(k, 0, up, y_send.at[0, k], y_recv.at[0, k])
            along(k, 0, down, y_send.at[1, k], y_recv.at[1, k])
            across(k, 0)
        k = turn - 2
        if 0 <= k < nz:
            drained(block(k, 3), y_recv.at[0, k])
            if k % 2 == 0:
                along(k, 3, up, f_send.at[k], f_recv.at[k])
            across(k, 3)
            drained(block(k, 1), y_recv.at[1, k])
            if k % 2 == 1:
                along(k, 1, down, f_send.at[k], f_recv.at[k])
            across(k, 1)
        if turn == nz + 2:
            forward(c, 3, False)
            forward(c, 1, False)
        k = turn - 3
        if 0 <= k < nz:
            drained(block(k, 2), f_recv.at[k])
            across(k, 2)
        if turn == nz // 2:
            gates()
        if turn == nz // 2 + 1:
            products()
        if turn == nz:
            for load in loads:
                load.wait()
            forward(c, 0, True)
            ring(0)
            for step in range(1, nx):
                drained(hid, h_recv.at[step - 1])
            remote(held.at[:, c], held.at[:, c], t_send, t_recv, other)
        if turn == nz + 2:
            ring(1)
    forward(c, 2, False)
    drained(xy.at[:, pl.ds(pl.multiple_of((1 - c) * half, cap), half), :], c_recv)
    for turn in range(4):
        forward(1 - c, turn, turn == 0)

    units = accs.shape[1]

    def activate(i, _):
        here = pl.ds(pl.multiple_of(i * 16, 16), 16)
        gate, wider, backed = accs[0, here, :], accs[1, here, :], accs[2, here, :]
        sig = jax.nn.sigmoid(gate)
        active = gate * sig
        acts[0, here, :] = (backed * wider * (sig * (1.0 + gate * (1.0 - sig)))).astype(BF16)
        acts[1, here, :] = (backed * active).astype(BF16)
        acts[2, here, :] = (active * wider).astype(BF16)
        return 0

    lax.fori_loop(0, units // 16, activate, 0)

    chunk = 2 * group
    chunks = nz // 2

    def step_rows(i):
        at = (chunks - 1 - i) * chunk
        lines = [
            pl.ds(pl.multiple_of(side * half + at, chunk), chunk) for side in (1 - c, c)
        ]
        left = [
            jnp.concatenate([jnp.transpose(acts[m, :, n]) for n in lines], axis=0)
            for m in range(2)
        ]

        def some(n, _):
            here = pl.ds(pl.multiple_of(n * width, 128), width)
            got = jnp.dot(left[0], wts[0, :, here], preferred_element_type=F32)
            got = got + jnp.dot(left[1], wts[1, :, here], preferred_element_type=F32)
            give_rows[pl.ds(at, chunk), here] = got[:chunk].astype(BF16)
            own_rows[pl.ds(at, chunk), here] = got[chunk:].astype(BF16)
            return 0

        lax.fori_loop(0, ny, some, 0)
        span_of = pl.ds(at, chunk)
        remote(give_rows.at[span_of], pair.at[span_of], p_send.at[i], p_recv.at[i], other)

    def step_pair(i):
        at = (chunks - 1 - i) * chunk
        span_of = pl.ds(at, chunk)
        drained(pair.at[span_of], p_recv.at[i])
        for turn in (2, 1, 3, 0):
            total = own_rows[span_of, cols(turn)].astype(F32)
            total = total + pair[span_of, cols(turn)].astype(F32)
            sums[turn, span_of, :] = total.astype(BF16)
        low, high = pl.ds(at, group), pl.ds(at + group, group)
        remote(sums.at[2, low], far.at[0, i], e_send.at[0, i], e_recv.at[0, i], up)
        remote(sums.at[2, high], far.at[1, i], e_send.at[1, i], e_recv.at[1, i], down)
        remote(sums.at[1, high], near.at[0, high], e_send.at[2, i], e_recv.at[2, i], up)
        remote(sums.at[3, low], near.at[1, low], e_send.at[3, i], e_recv.at[3, i], down)

    def step_far(i):
        at = (chunks - 1 - i) * chunk
        low, high = pl.ds(at, group), pl.ds(at + group, group)
        for side, turn, where, to in ((0, 1, low, up), (1, 3, high, down)):
            drained(far.at[side, i], e_recv.at[side, i])
            total = sums[turn, where, :].astype(F32) + far[side, i].astype(F32)
            sums[turn, where, :] = total.astype(BF16)
            remote(
                sums.at[turn, where], near.at[side, where], e_send.at[4 + side, i],
                e_recv.at[4 + side, i], to,
            )

    def give(i, _):
        k, sx = i // nx, lax.rem(x + lax.rem(i, nx), nx)
        to = (lax.rem(z + nz - offset_of(k, nz), nz), sx, c, y)
        remote(
            mine.at[pl.ds(pl.multiple_of((k * nx + sx) * cap, cap), cap), :],
            back.at[mine_too, :],
            r_send, r_recv, to,
        )
        return 0

    def step_near(i):
        at = (chunks - 1 - i) * chunk
        span_of = pl.ds(at, chunk)
        for n in range(2, 6):
            drained(far.at[0, i], e_recv.at[n, i])
        total = sums[0, span_of, :].astype(F32) + near[0, span_of, :].astype(F32)
        mine[span_of, :] = (total + near[1, span_of, :].astype(F32)).astype(BF16)
        k = (chunks - 1 - i) * 2
        if k == 0:
            back[mine_too, :] = mine[pl.ds(pl.multiple_of(x * cap, cap), cap), :]
        lax.fori_loop(max(k * nx, 1), (k + 2) * nx, give, 0)

    tall = 256

    def weight_grad(m):
        def some(i, _):
            here = pl.ds(pl.multiple_of(i * tall, tall), tall)
            grads[m, :, here] = jnp.dot(
                acts[m], xy[m // 2, :, here], preferred_element_type=F32
            ).astype(BF16)
            return 0

        lax.fori_loop(0, feats // tall, some, 0)
        pltpu.make_async_copy(grads.at[m], outs[m], out_sem.at[m]).start()

    later_rings = list(range(2, rounds + 1))
    step_rows(0)
    for i in range(1, chunks):
        step_rows(i)
        step_pair(i - 1)
    step_pair(chunks - 1)
    todo = 0
    for i in range(chunks):
        step_far(i)
        if later_rings:
            ring(later_rings.pop(0))
        if i >= 1:
            if todo < 3:
                weight_grad(todo)
                todo += 1
            step_near(i - 1)
    while todo < 3:
        weight_grad(todo)
        todo += 1
    step_near(chunks - 1)
    for s in later_rings:
        ring(s)
    weigh_all()

    slot = lax.broadcasted_iota(jnp.int32, (toks, half), 1)
    chosen = (slot == spots[:, 0:1]) | (slot == spots[:, 1:2])
    onehot = jnp.where(chosen, 1.0, 0.0).astype(BF16)
    drained(back.at[pl.ds(0, half - cap), :], r_recv)
    moe[:, cols(0)] = jnp.dot(onehot, back[...], preferred_element_type=F32).astype(BF16)
    for step in (1, 3, 2):
        remote(
            moe.at[:, cols(0)], moe.at[:, cols(0)], m_send.at[step - 1], m_recv.at[step - 1],
            (z, x, c, lax.rem(y + step, ny)),
        )
    drained(wide.at[:, :, 1 - c], s_recv)
    drained(held.at[:, 1 - c], t_recv)
    for step in (1, 3, 2):
        drained(moe.at[:, cols(ny - step)], m_recv.at[step - 1])
    mixed[...] = (cot[...].astype(F32) + moe[...].astype(F32)).astype(BF16)

    lines = rmap.shape[0]
    turned[...] = jnp.transpose(mixed[...]).reshape(nz, 2 * nx, lines, toks)
    spot = x * 2 + c
    ours = pl.ds(pl.multiple_of(spot * toks, toks), toks)
    cross[:, :, ours] = turned[:, spot]
    for step in range(1, 2 * nx):
        to = lax.rem(spot + step, 2 * nx)
        remote(
            turned.at[:, to], cross.at[:, :, ours], g_send.at[step - 1], g_recv.at[step - 1],
            (z, to // 2, lax.rem(to, 2), y),
        )

    state = jnp.dot(mixed[...], wide[...].reshape(-1, width), preferred_element_type=F32)
    for n, s in enumerate(reach):
        state = state + levels[n] * pltpu.roll(state, toks - s, 0)
    first = pieces[4, 0:1, :] * state[0:1]
    for i in range(width // 128):
        small[1, pl.ds(i, 1), :] = first[:, i * 128 : (i + 1) * 128]
    alphas[index] = small[1]
    tell(small.at[1], alphas, a_send.at[1], a_recv.at[1])

    for step in range(1, 2 * nx):
        drained(turned.at[:, 0], g_recv.at[step - 1])
    total = jnp.dot(
        cross[...].reshape(nz * lines, 2 * nx * toks),
        held[...].reshape(2 * nx * toks, width),
        preferred_element_type=F32,
    )
    fold[...] = total.astype(BF16).reshape(nz, lines, width)
    rest[z] = fold[z]
    for step in range(1, nz):
        to = lax.rem(z + step, nz)
        remote(fold.at[to], rest.at[z], q_send.at[step - 1], q_recv.at[step - 1], (to, x, c, y))

    drained(alphas.at[pl.ds(0, plane - 1)], a_recv.at[1])
    carried = jnp.sum(weights[...] * alphas[...], axis=0)
    carried = jnp.concatenate([carried[i : i + 1] for i in range(width // 128)], axis=1)
    state = state + pieces[3] * carried
    grad_rec = (state * pieces[0]).astype(BF16)
    grad_in = (state * pieces[1]).astype(BF16)
    direct = state * pieces[2]
    for b in range(blocks):
        here = slice(b * span, (b + 1) * span)
        lru_out[:, here] = (
            direct[:, here]
            + lax.dot_general(grad_rec[:, here], rtile[b], turn_dims, preferred_element_type=F32)
            + lax.dot_general(grad_in[:, here], itile[b], turn_dims, preferred_element_type=F32)
        )

    for step in range(1, nz):
        drained(fold.at[0], q_recv.at[step - 1])
    summed = rest[0].astype(F32)
    for i in range(1, nz):
        summed = summed + rest[i].astype(F32)
    proj_out[...] = summed

    whole = xy.at[:, pl.ds(pl.multiple_of(c * half, cap), half), :]
    drained(whole, c_send)
    drained(slots.at[:, pl.ds(0, half - cap), :], d_send)
    for k in range(nz):
        drained(block(k, 0), y_send.at[0, k])
        drained(block(k, 0), y_send.at[1, k])
        drained(block(k, 2), f_send.at[k])
    for i in range(chunks):
        drained(pair.at[pl.ds(0, chunk)], p_send.at[i])
        for n in range(6):
            drained(far.at[0, 0], e_send.at[n, i])
    drained(back.at[pl.ds(0, half - cap), :], r_send)
    for step in (1, 2, 3):
        drained(moe.at[:, cols(0)], m_send.at[step - 1])
    for step in range(nx - 1):
        drained(rmap, b_send.at[step])
        drained(hid, h_send.at[step])
    for s in range(rounds):
        for side in range(2):
            drained(ring_sent(s, side), z_send.at[side, s])
    drained(wide.at[:, :, c], s_send)
    drained(held.at[:, c], t_send)
    for i in range(2):
        drained(betas.at[pl.ds(0, plane - 1)], a_send.at[i])
    for step in range(2 * nx - 1):
        drained(turned.at[:, 0], g_send.at[step])
    for step in range(nz - 1):
        drained(fold.at[0], q_send.at[step])
    for m in range(3):
        pltpu.make_async_copy(grads.at[m], outs[m], out_sem.at[m]).wait()


def layer_entry(dims, cap, *refs):
    layer_kernel(dims, cap, *refs[:12], refs[12:15], refs[15:18], *refs[18:])


def layer(dims, cap, *operands):
    target, spots, share, cot, rows, rmap, xmem, hid, fade, extra, rtile, itile, *maps = operands
    nz, nx, ny = dims
    toks, feats = cot.shape
    half, width, group = nz * nx * cap, feats // ny, nx * cap
    lines, units = rmap.shape[0], maps[0].shape[0]
    plane, lanes, steps = nz * nx * 2, width // 128, toks.bit_length() - 1
    vmem, anyw = pl.BlockSpec(memory_space=pltpu.VMEM), pl.BlockSpec(memory_space=pl.ANY)
    dma = pltpu.SemaphoreType.DMA
    return pl.pallas_call(
        functools.partial(layer_entry, dims, cap),
        out_shape=[jax.ShapeDtypeStruct((units, feats), BF16)] * 3
        + [
            jax.ShapeDtypeStruct((lines, width), F32),
            jax.ShapeDtypeStruct((toks, width), F32),
        ],
        in_specs=[vmem] * 12 + [anyw] * 3,
        out_specs=[anyw] * 3 + [vmem] * 2,
        scratch_shapes=[
            pltpu.VMEM((2, half, width), BF16),
            pltpu.VMEM((2, 2 * half, feats), BF16),
            pltpu.VMEM((3, units, feats), BF16),
            pltpu.VMEM((3, units, 2 * half), F32),
            pltpu.VMEM((3, units, 2 * half), BF16),
            pltpu.VMEM((half, feats), BF16),
            pltpu.VMEM((half, feats), BF16),
            pltpu.VMEM((half, feats), BF16),
            pltpu.VMEM((4, half, width), BF16),
            pltpu.VMEM((2, nz // 2, group, width), BF16),
            pltpu.VMEM((2, half, width), BF16),
            pltpu.VMEM((half, width), BF16),
            pltpu.VMEM((half, width), BF16),
            pltpu.VMEM((toks, feats), BF16),
            pltpu.VMEM((toks, feats), BF16),
            pltpu.VMEM((3, units, feats), BF16),
            pltpu.VMEM((nz, nx, 2, lines, width), BF16),
            pltpu.VMEM((nx, 2, toks, width), BF16),
            pltpu.VMEM((nz, 2 * nx, lines, toks), BF16),
            pltpu.VMEM((nz, lines, 2 * nx * toks), BF16),
            pltpu.VMEM((nz, lines, width), BF16),
            pltpu.VMEM((nz, lines, width), BF16),
            pltpu.VMEM((steps, toks, width), F32),
            pltpu.VMEM((5, toks, width), F32),
            pltpu.VMEM((plane, lanes, 128), F32),
            pltpu.VMEM((plane, lanes, 128), F32),
            pltpu.VMEM((plane, lanes, 128), F32),
            pltpu.VMEM((2, lanes, 128), F32),
            dma, dma((3,)), dma((3,)),
            dma, dma((nz,)), dma((2, nz)), dma((2, nz)), dma((nz,)), dma((nz,)), dma, dma,
            dma((nz // 2,)), dma((nz // 2,)), dma((6, nz // 2)), dma((6, nz // 2)), dma, dma,
            dma((3,)), dma((3,)), dma((nx - 1,)), dma((nx - 1,)), dma((2, nz // 2)),
            dma((2, nz // 2)), dma, dma, dma((nx - 1,)), dma((nx - 1,)), dma, dma, dma((2,)),
            dma((2,)), dma((2 * nx - 1,)), dma((2 * nx - 1,)), dma((nz - 1,)), dma((nz - 1,)),
        ],
        compiler_params=pltpu.CompilerParams(
            collective_id=0, has_side_effects=True, vmem_limit_bytes=60 * 2**20
        ),
        name="layer",
    )(*operands)


def local(
    result_cotangent_values,
    specialist_entry_vectors,
    chosen_specialists,
    specialist_mixing_shares,
    specialist_switch_maps,
    specialist_widen_maps,
    specialist_shrink_maps,
    memory_readout_map,
    memory_source_vectors,
    memory_hidden_values,
    feature_fading_speed,
    extra_log_fading,
    memory_switch_tiles,
    entry_switch_tiles,
):
    tok_rows, feature_count = result_cotangent_values.shape
    route_count = chosen_specialists.shape[1]
    sp_count = lax.axis_size(SP)
    expert_count = sp_count // SLICES
    capacity = min(tok_rows, 4 * tok_rows // expert_count)
    pairs = chosen_specialists.T.reshape(-1)
    order = (jnp.arange(tok_rows)[None, :] * route_count + jnp.arange(route_count)[:, None]).reshape(-1)
    earlier = (pairs[:, None] == pairs[None, :]) & (order[:, None] < order[None, :])
    target = pairs * capacity + jnp.sum(earlier.astype(jnp.int32), axis=0)
    dims = (lax.axis_size("sp_0"), lax.axis_size("sp_1"), lax.axis_size("tp"))
    gate_weight_grad, up_weight_grad, down_grad, out_proj_grad, lru_input_grad = layer(
        dims,
        capacity,
        target[None, :],
        target.reshape(route_count, tok_rows).T,
        specialist_mixing_shares,
        result_cotangent_values,
        specialist_entry_vectors,
        memory_readout_map,
        memory_source_vectors,
        memory_hidden_values,
        feature_fading_speed[None, :],
        extra_log_fading[:, None],
        memory_switch_tiles,
        entry_switch_tiles,
        specialist_switch_maps[0].T,
        specialist_widen_maps[0].T,
        specialist_shrink_maps[0],
    )
    return (
        gate_weight_grad.T[None],
        up_weight_grad.T[None],
        down_grad[None],
        out_proj_grad,
        lru_input_grad,
    )


def solution(mesh):
    finer = Mesh(mesh.devices.reshape(8, 4, 2, mesh.shape["tp"]), ("sp_0", "sp_1", "sp_2", "tp"))
    in_specs = (
        P(SP, None),
        P(SP, None),
        P(SP, None),
        P(SP, None),
        P(SP, None, "tp"),
        P(SP, None, "tp"),
        P(SP, "tp", None),
        P(SP, "tp"),
        P(SP, "tp"),
        P(SP, "tp"),
        P("tp"),
        P(SP),
        P("tp", None, None),
        P("tp", None, None),
    )
    out_specs = (P(SP, None, "tp"), P(SP, None, "tp"), P(SP, "tp", None), P(SP, "tp"), P(SP, "tp"))
    return jax.shard_map(local, mesh=finer, in_specs=in_specs, out_specs=out_specs, check_vma=False)
```

time: 170 us -> 152 us (0.89)
  matrix products: 18.9 us -> 0 us
    dot_general x5 -> x0, matrix products: 18.9 us -> none  [the longest x1 5 us: expert_backward(): jnp.dot(inputs, gate_weight, preferred_element_type=jnp.float32)]
    pallas_call x2 -> x1, Pallas kernels: 137 us -> 138 us  [layer(): pl.pallas_call(functools.partial(layer_entry, dims, cap), out_shape=[jax....]
    unnamed x25 -> x15, local copies, waits for them, and re-layouts: 10.8 us -> 10 us
where the time goes in v2:
time: 152 us
  Pallas kernels  138 us (91%)
  local copies, waits for them, and re-layouts  11.6 us (8%)
    pallas_call x1, Pallas kernels, layer(): pl.pallas_call(functools.partial(layer_entry, dims, cap), out_shape=[jax....  138 us
    unnamed x15, local copies, waits for them, and re-layouts  10 us

profile of v2, /device:TPU:1, one launch (start us, length us, event | category | flops | bytes accessed | tf_op | source)
XLA Modules:
  0.0 151.8 jit_solution(11637691523732359060)
XLA Ops:
  0.7 0.8 copy.34
  1.4 0.1 copy.37
  1.5 0.2 convert_reduce_fusion
  1.7 0.1 copy.38
  1.8 0.6 add_bitcast_fusion
  2.4 0.1 copy.36
  2.5 0.6 add.41.refs_0_
  3.1 1.4 copy.39.refs_2_
  4.5 1.4 copy.40.refs_9_
  5.9 138.1 %layer.1 = (bf16[448,2048]{1,0:T(8,128)(2,1)}, bf16[448,2048]{1,0:T(8,128)(2,1)}, bf16[448,2048]{1,0:T(8,128)(2,1)}, f32[32,512]{1,0:T(8,128)}, f32[128,512]{1,0:T(8,128)}) custom-call(s32[1,256]{1,0:T(1,128)} %add.41.refs_0_, s32[128,2]{1,0:T(8,128)} %get-tuple-element.15.refs_1_, f32[128,2]{1,0:T(8,128)} %copy.39.refs_2_, bf16[128,2048]{1,0:T(8,128)(2,1)} %refs_3_.1, ...), custom_call_target="tpu_custom_call" | custom-call | tf_op jit(solution)/shard_map/layer/pallas_call | solution.py:515
  143.9 0.0 copy-start.1
  144.0 3.1 %copy.46 = bf16[1,2048,448]{1,2,0:T(8,128)(2,1)} copy(bf16[1,2048,448]{1,2,0:T(8,128)(2,1)} %bitcast.30) | data formatting | bytes 3670016
  147.0 0.0 copy-done.1
  147.0 0.0 copy-start
  147.0 1.2 copy.47
  148.3 0.9 copy-done
  149.2 0.0 copy-start.3
  149.2 0.0 copy-start.2
  149.2 1.2 copy.48
  150.4 0.0 copy-done.3
  150.4 0.6 copy.49
  151.1 0.0 copy-done.2
  151.1 0.7 copy.50
  (2 shorter events, 0.0 us)
Async XLA Ops:
  143.9 3.1 %copy-start.1 = (bf16[448,2048]{1,0:T(8,128)(2,1)S(1)}, bf16[448,2048]{1,0:T(8,128)(2,1)}, u32[]{:S(2)}) copy-start(bf16[448,2048]{1,0:T(8,128)(2,1)} %get-tuple-element.11) | copy-start | bytes 5505028
  147.0 2.2 %copy-start = (bf16[448,2048]{1,0:T(8,128)(2,1)S(1)}, bf16[448,2048]{1,0:T(8,128)(2,1)}, u32[]{:S(2)}) copy-start(bf16[448,2048]{1,0:T(8,128)(2,1)} %get-tuple-element.12) | copy-start | bytes 5505028
  149.2 1.2 copy-start.3
  149.2 1.9 %copy-start.2 = (f32[128,512]{1,0:T(8,128)S(1)}, f32[128,512]{1,0:T(8,128)}, u32[]{:S(2)}) copy-start(f32[128,512]{1,0:T(8,128)} %get-tuple-element.26) | copy-start | bytes 786436

commit v3 on v2

--- a/solution.py
+++ b/solution.py
@@ -28,11 +28,11 @@
 
 
 def layer_kernel(
-    dims, cap, target, spots, share, cot, rows, rmap, xmem, hid, fade, extra, rtile, itile, maps,
+    dims, cap, chosen, share, cot, rows, rmap, xmem, hid, fade, extra, rtile, itile, maps,
     outs, proj_out, lru_out,
-    slots, xy, wts, accs, acts, give_rows, own_rows, pair, sums, far, near, back, mine, moe, mixed,
-    grads, wide, held, turned, cross, fold, rest, levels, pieces, alphas, betas, weights, small,
-    own_sem, in_sem, out_sem, d_send, d_recv, y_send, y_recv, f_send, f_recv, c_send, c_recv,
+    slots, xy, wts, flipped, accs, acts, across_acts, give_rows, own_rows, pair, sums, far, near, back, mine, moe, mixed,
+    wide, held, turned, cross, fold, rest, levels, pieces, alphas, betas, weights, small, picked,
+    in_sem, out_sem, d_send, d_recv, y_send, y_recv, f_send, f_recv, c_send, c_recv,
     p_send, p_recv, e_send, e_recv, r_send, r_recv, m_send, m_recv, b_send, b_recv, z_send, z_recv,
     s_send, s_recv, h_send, h_recv, t_send, t_recv, a_send, a_recv, g_send, g_recv, q_send, q_recv,
 ):
@@ -77,17 +77,36 @@
     wide[z, x, c] = rmap[...]
     held[x, c] = hid[...]
 
-    slot = lax.broadcasted_iota(jnp.int32, (half, target.shape[1]), 0)
-    onehot = jnp.where(slot == target[...], 1.0, 0.0).astype(BF16)
+    def upright(line):
+        return jnp.transpose(jnp.broadcast_to(line, (toks, toks)))
+
+    experts = [chosen[k : k + 1, :].astype(F32) for k in range(2)]
+    earlier = [
+        lax.broadcasted_iota(jnp.int32, (toks, toks), 0)
+        < lax.broadcasted_iota(jnp.int32, (toks, toks), 1) + k
+        for k in range(2)
+    ]
+    places = []
+    for k in range(2):
+        rank = jnp.zeros((1, toks), F32)
+        for j in range(2):
+            same = (upright(experts[j]) == experts[k]) & earlier[1 if j < k else 0]
+            rank = rank + jnp.sum(jnp.where(same, 1.0, 0.0), axis=0, keepdims=True)
+        places.append(experts[k] * cap + rank)
+    slot = lax.broadcasted_iota(jnp.int32, (half, 2 * toks), 0).astype(F32)
+    onehot = jnp.where(slot == jnp.concatenate(places, axis=1), 1.0, 0.0).astype(BF16)
     some = rows[:, cols(0)]
     slots[0] = jnp.dot(
         onehot, jnp.concatenate([some, some], axis=0), preferred_element_type=F32
     ).astype(BF16)
     some = cot[:, cols(0)].astype(F32)
-    scaled = [(share[:, k : k + 1] * some).astype(BF16) for k in range(2)]
+    scaled = [(upright(share[k : k + 1, :])[:, 0:1] * some).astype(BF16) for k in range(2)]
     slots[1] = jnp.dot(
         onehot, jnp.concatenate(scaled, axis=0), preferred_element_type=F32
     ).astype(BF16)
+    slot = lax.broadcasted_iota(jnp.int32, (toks, half), 1).astype(F32)
+    found = [slot == upright(places[k])[:, 0:1] for k in range(2)]
+    picked[...] = jnp.where(found[0] | found[1], 1.0, 0.0).astype(BF16)
 
     def source(e):
         return slots.at[:, pl.ds(pl.multiple_of(e * cap, cap), cap), :]
@@ -102,17 +121,28 @@
         xy[i, here, cols(0)] = slots[i, mine_too, :]
     pl.semaphore_wait(barrier, plane - 1 + 3)
 
-    def push(i, _):
-        k, dx = i // nx, lax.rem(i, nx)
-        tz, tx = lax.rem(z + offset_of(k, nz), nz), lax.rem(x + dx, nx)
-        remote(source(tz * nx + tx), landing(k), d_send, d_recv.at[k], (tz, tx, c, y))
-        return 0
-
-    lax.fori_loop(1, nz * nx, push, 0)
-    for step in range(1, nx):
-        to = (z, lax.rem(x + step, nx), c, y)
-        remote(rmap, wide.at[z, x, c], b_send.at[step - 1], b_recv.at[step - 1], to)
-        remote(hid, held.at[x, c], h_send.at[step - 1], h_recv.at[step - 1], to)
+    def push(k):
+        def one(dx, _):
+            tz, tx = lax.rem(z + offset_of(k, nz), nz), lax.rem(x + dx, nx)
+            remote(source(tz * nx + tx), landing(k), d_send, d_recv.at[k], (tz, tx, c, y))
+            return 0
+
+        lax.fori_loop(1 if k == 0 else 0, nx, one, 0)
+
+    ahead = 3
+    for k in range(ahead):
+        push(k)
+
+    def push_rest():
+        for step in range(1, nx):
+            to = (z, lax.rem(x + step, nx), c, y)
+            remote(rmap, wide.at[z, x, c], b_send.at[step - 1], b_recv.at[step - 1], to)
+            remote(hid, held.at[x, c], h_send.at[step - 1], h_recv.at[step - 1], to)
+
+    def hand_over():
+        for step in range(1, nx):
+            drained(hid, h_recv.at[step - 1])
+        remote(held.at[:, c], held.at[:, c], t_send, t_recv, other)
 
     rounds = nz // 2
 
@@ -153,7 +183,7 @@
             rec = jax.nn.sigmoid(jnp.dot(some, rtile[b], preferred_element_type=F32))
             inp = jax.nn.sigmoid(jnp.dot(some, itile[b], preferred_element_type=F32))
             speed = -8.0 * fade[:, here]
-            log_decay = rec * speed + extra[...]
+            log_decay = rec * speed + upright(extra[...])[:, 0:1]
             decay = jnp.exp(log_decay)
             spare = 1.0 - jnp.exp(2.0 * log_decay)
             scale = jnp.sqrt(jnp.maximum(spare, 0.01))
@@ -201,102 +231,68 @@
         return xy.at[:, pl.ds(start, group), cols(turn)]
 
     def across(k, turn):
-        remote(block(k, turn), block(k, turn), c_send, c_recv, other)
+        remote(block(k, turn), block(k, turn), c_send, c_recv.at[k // (nz // 2), turn], other)
 
     def along(k, turn, to, send, recv):
         remote(block(k, turn), block(k, turn), send, recv, to)
 
     turn_dims = (((1,), (1,)), ((), ()))
-    piece = min(256, half)
-
-    def forward(side, turn, first):
+    piece = half // 2
+    units = accs.shape[2]
+
+    def flip(m):
+        loads[m].wait()
+
         def some(i, _):
-            m, n = i // (half // piece), lax.rem(i, half // piece)
-            here = pl.ds(pl.multiple_of(side * half + n * piece, cap), piece)
-            got = lax.dot_general(
-                wts[m, :, cols(turn)], xy[m // 2, here, cols(turn)], turn_dims,
-                preferred_element_type=F32,
+            here = pl.ds(pl.multiple_of(i * 128, 128), 128)
+            flipped[m, here, :] = jnp.transpose(wts[m, :, here])
+            return 0
+
+        lax.fori_loop(0, feats // 128, some, 0)
+
+    def forward(own, part, turn):
+        side = c if own else 1 - c
+        here = pl.ds(pl.multiple_of(side * half + part * piece, cap), piece)
+        if not own:
+            drained(xy.at[:, here, cols(turn)], c_recv.at[part, turn])
+
+        def some(m, _):
+            got = jnp.dot(
+                xy[m // 2, here, cols(turn)], flipped[m, cols(turn), :], preferred_element_type=F32
             )
-            if first:
-                accs[m, :, here] = got
+            if turn == 0:
+                accs[m, here, :] = got
             else:
-                accs[m, :, here] += got
-            return 0
-
-        lax.fori_loop(0, 3 * (half // piece), some, 0)
-
-    for turn in range(nz + 3):
-        k = turn
-        if k < nz:
-            if k == 0:
-                drained(slots.at[:, pl.ds(0, group - cap), :], d_recv.at[0])
-            else:
-                drained(block(k, 0), d_recv.at[k])
-            along(k, 0, up, y_send.at[0, k], y_recv.at[0, k])
-            along(k, 0, down, y_send.at[1, k], y_recv.at[1, k])
-            across(k, 0)
-        k = turn - 2
-        if 0 <= k < nz:
-            drained(block(k, 3), y_recv.at[0, k])
-            if k % 2 == 0:
-                along(k, 3, up, f_send.at[k], f_recv.at[k])
-            across(k, 3)
-            drained(block(k, 1), y_recv.at[1, k])
-            if k % 2 == 1:
-                along(k, 1, down, f_send.at[k], f_recv.at[k])
-            across(k, 1)
-        if turn == nz + 2:
-            forward(c, 3, False)
-            forward(c, 1, False)
-        k = turn - 3
-        if 0 <= k < nz:
-            drained(block(k, 2), f_recv.at[k])
-            across(k, 2)
-        if turn == nz // 2:
-            gates()
-        if turn == nz // 2 + 1:
-            products()
-        if turn == nz:
-            for load in loads:
-                load.wait()
-            forward(c, 0, True)
-            ring(0)
-            for step in range(1, nx):
-                drained(hid, h_recv.at[step - 1])
-            remote(held.at[:, c], held.at[:, c], t_send, t_recv, other)
-        if turn == nz + 2:
-            ring(1)
-    forward(c, 2, False)
-    drained(xy.at[:, pl.ds(pl.multiple_of((1 - c) * half, cap), half), :], c_recv)
-    for turn in range(4):
-        forward(1 - c, turn, turn == 0)
-
-    units = accs.shape[1]
-
-    def activate(i, _):
-        here = pl.ds(pl.multiple_of(i * 16, 16), 16)
-        gate, wider, backed = accs[0, here, :], accs[1, here, :], accs[2, here, :]
-        sig = jax.nn.sigmoid(gate)
-        active = gate * sig
-        acts[0, here, :] = (backed * wider * (sig * (1.0 + gate * (1.0 - sig)))).astype(BF16)
-        acts[1, here, :] = (backed * active).astype(BF16)
-        acts[2, here, :] = (active * wider).astype(BF16)
-        return 0
-
-    lax.fori_loop(0, units // 16, activate, 0)
+                accs[m, here, :] += got
+            return 0
+
+        lax.fori_loop(0, 3, some, 0)
+
+    def activate(part):
+        tile = 16
+
+        def some(i, _):
+            side, n = i // (piece // tile), lax.rem(i, piece // tile)
+            here = pl.ds(pl.multiple_of(side * half + part * piece + n * tile, tile), tile)
+            gate, wider, backed = accs[0, here, :], accs[1, here, :], accs[2, here, :]
+            sig = jax.nn.sigmoid(gate)
+            active = gate * sig
+            acts[0, here, :] = (backed * wider * (sig * (1.0 + gate * (1.0 - sig)))).astype(BF16)
+            acts[1, here, :] = (backed * active).astype(BF16)
+            acts[2, here, :] = (active * wider).astype(BF16)
+            return 0
+
+        lax.fori_loop(0, 2 * (piece // tile), some, 0)
 
     chunk = 2 * group
     chunks = nz // 2
 
     def step_rows(i):
-        at = (chunks - 1 - i) * chunk
+        at = i * chunk
         lines = [
             pl.ds(pl.multiple_of(side * half + at, chunk), chunk) for side in (1 - c, c)
         ]
-        left = [
-            jnp.concatenate([jnp.transpose(acts[m, :, n]) for n in lines], axis=0)
-            for m in range(2)
-        ]
+        left = [jnp.concatenate([acts[m, n, :] for n in lines], axis=0) for m in range(2)]
 
         def some(n, _):
             here = pl.ds(pl.multiple_of(n * width, 128), width)
@@ -311,7 +307,7 @@
         remote(give_rows.at[span_of], pair.at[span_of], p_send.at[i], p_recv.at[i], other)
 
     def step_pair(i):
-        at = (chunks - 1 - i) * chunk
+        at = i * chunk
         span_of = pl.ds(at, chunk)
         drained(pair.at[span_of], p_recv.at[i])
         for turn in (2, 1, 3, 0):
@@ -325,7 +321,7 @@
         remote(sums.at[3, low], near.at[1, low], e_send.at[3, i], e_recv.at[3, i], down)
 
     def step_far(i):
-        at = (chunks - 1 - i) * chunk
+        at = i * chunk
         low, high = pl.ds(at, group), pl.ds(at + group, group)
         for side, turn, where, to in ((0, 1, low, up), (1, 3, high, down)):
             drained(far.at[side, i], e_recv.at[side, i])
@@ -347,13 +343,13 @@
         return 0
 
     def step_near(i):
-        at = (chunks - 1 - i) * chunk
+        at = i * chunk
         span_of = pl.ds(at, chunk)
         for n in range(2, 6):
             drained(far.at[0, i], e_recv.at[n, i])
         total = sums[0, span_of, :].astype(F32) + near[0, span_of, :].astype(F32)
         mine[span_of, :] = (total + near[1, span_of, :].astype(F32)).astype(BF16)
-        k = (chunks - 1 - i) * 2
+        k = i * 2
         if k == 0:
             back[mine_too, :] = mine[pl.ds(pl.multiple_of(x * cap, cap), cap), :]
         lax.fori_loop(max(k * nx, 1), (k + 2) * nx, give, 0)
@@ -361,50 +357,114 @@
     tall = 256
 
     def weight_grad(m):
+        def turn_over(i, _):
+            here = pl.ds(pl.multiple_of(i * 128, 128), 128)
+            across_acts[:, here] = jnp.transpose(acts[m, here, :])
+            return 0
+
+        lax.fori_loop(0, 2 * half // 128, turn_over, 0)
+
         def some(i, _):
             here = pl.ds(pl.multiple_of(i * tall, tall), tall)
-            grads[m, :, here] = jnp.dot(
-                acts[m], xy[m // 2, :, here], preferred_element_type=F32
+            wts[m, :, here] = jnp.dot(
+                across_acts[...], xy[m // 2, :, here], preferred_element_type=F32
             ).astype(BF16)
             return 0
 
         lax.fori_loop(0, feats // tall, some, 0)
-        pltpu.make_async_copy(grads.at[m], outs[m], out_sem.at[m]).start()
-
+        pltpu.make_async_copy(wts.at[m], outs[m], out_sem.at[m]).start()
+
+    def receive(k):
+        if k == 0:
+            drained(slots.at[:, pl.ds(0, group - cap), :], d_recv.at[0])
+        else:
+            drained(block(k, 0), d_recv.at[k])
+        along(k, 0, up, y_send.at[0, k], y_recv.at[0, k])
+        along(k, 0, down, y_send.at[1, k], y_recv.at[1, k])
+        across(k, 0)
+        if k + ahead < nz:
+            push(k + ahead)
+
+    def receive_near(k):
+        drained(block(k, 3), y_recv.at[0, k])
+        if k % 2 == 0:
+            along(k, 3, up, f_send.at[k], f_recv.at[k])
+        across(k, 3)
+        drained(block(k, 1), y_recv.at[1, k])
+        if k % 2 == 1:
+            along(k, 1, down, f_send.at[k], f_recv.at[k])
+        across(k, 1)
+
+    def receive_far(k):
+        drained(block(k, 2), f_recv.at[k])
+        across(k, 2)
+
+    def work(what, *args):
+        return functools.partial(what, *args)
+
+    mid = nz // 2
+    fillers = {}
+    for at, jobs in (
+        (0, [work(flip, 0), work(flip, 2)]),
+        (1, [work(flip, 1), work(gates)]),
+        (2, [work(products)]),
+        (3, [work(push_rest)]),
+        (mid, [work(forward, True, 0, 0)]),
+        (mid + 1, [work(forward, False, 0, 0), work(forward, True, 0, 3)]),
+        (mid + 2, [work(forward, True, 0, 1), work(forward, False, 0, 3)]),
+        (mid + 3, [work(forward, True, 0, 2), work(forward, False, 0, 1)]),
+        (nz, [work(forward, False, 0, 2), work(ring, 0), work(forward, True, 1, 0)]),
+        (nz + 1, [work(activate, 0), work(hand_over), work(step_rows, 0),
+                  work(forward, False, 1, 0), work(forward, True, 1, 3)]),
+        (nz + 2, [work(step_rows, 1), work(forward, True, 1, 1), work(forward, False, 1, 3)]),
+    ):
+        fillers.setdefault(at, []).extend(jobs)
+    for turn in range(nz + 3):
+        if turn < nz:
+            receive(turn)
+        if 0 <= turn - 2 < nz:
+            receive_near(turn - 2)
+        if 0 <= turn - 3 < nz - 1:
+            receive_far(turn - 3)
+        for job in fillers.get(turn, []):
+            job()
+    receive_far(nz - 1)
+    early = chunks // 2
+    for i in range(early):
+        step_pair(i)
+    ring(1)
+    forward(False, 1, 1)
+    forward(True, 1, 2)
+    forward(False, 1, 2)
+    activate(1)
     later_rings = list(range(2, rounds + 1))
-    step_rows(0)
-    for i in range(1, chunks):
-        step_rows(i)
-        step_pair(i - 1)
-    step_pair(chunks - 1)
-    todo = 0
-    for i in range(chunks):
+    for i in range(early):
+        step_rows(early + i)
         step_far(i)
+    for i in range(early):
+        step_pair(early + i)
+        step_near(i)
+    if later_rings:
+        ring(later_rings.pop(0))
+    for i in range(early):
+        step_far(early + i)
+    for i in range(early):
         if later_rings:
             ring(later_rings.pop(0))
-        if i >= 1:
-            if todo < 3:
-                weight_grad(todo)
-                todo += 1
-            step_near(i - 1)
-    while todo < 3:
-        weight_grad(todo)
-        todo += 1
-    step_near(chunks - 1)
+        step_near(early + i)
+    weight_grad(0)
     for s in later_rings:
         ring(s)
     weigh_all()
 
-    slot = lax.broadcasted_iota(jnp.int32, (toks, half), 1)
-    chosen = (slot == spots[:, 0:1]) | (slot == spots[:, 1:2])
-    onehot = jnp.where(chosen, 1.0, 0.0).astype(BF16)
     drained(back.at[pl.ds(0, half - cap), :], r_recv)
-    moe[:, cols(0)] = jnp.dot(onehot, back[...], preferred_element_type=F32).astype(BF16)
+    moe[:, cols(0)] = jnp.dot(picked[...], back[...], preferred_element_type=F32).astype(BF16)
     for step in (1, 3, 2):
         remote(
             moe.at[:, cols(0)], moe.at[:, cols(0)], m_send.at[step - 1], m_recv.at[step - 1],
             (z, x, c, lax.rem(y + step, ny)),
         )
+    weight_grad(1)
     drained(wide.at[:, :, 1 - c], s_recv)
     drained(held.at[:, 1 - c], t_recv)
     for step in (1, 3, 2):
@@ -460,6 +520,7 @@
             + lax.dot_general(grad_in[:, here], itile[b], turn_dims, preferred_element_type=F32)
         )
 
+    weight_grad(2)
     for step in range(1, nz):
         drained(fold.at[0], q_recv.at[step - 1])
     summed = rest[0].astype(F32)
@@ -496,15 +557,15 @@
     for step in range(nz - 1):
         drained(fold.at[0], q_send.at[step])
     for m in range(3):
-        pltpu.make_async_copy(grads.at[m], outs[m], out_sem.at[m]).wait()
+        pltpu.make_async_copy(wts.at[m], outs[m], out_sem.at[m]).wait()
 
 
 def layer_entry(dims, cap, *refs):
-    layer_kernel(dims, cap, *refs[:12], refs[12:15], refs[15:18], *refs[18:])
+    layer_kernel(dims, cap, *refs[:11], refs[11:14], refs[14:17], *refs[17:])
 
 
 def layer(dims, cap, *operands):
-    target, spots, share, cot, rows, rmap, xmem, hid, fade, extra, rtile, itile, *maps = operands
+    chosen, share, cot, rows, rmap, xmem, hid, fade, extra, rtile, itile, *maps = operands
     nz, nx, ny = dims
     toks, feats = cot.shape
     half, width, group = nz * nx * cap, feats // ny, nx * cap
@@ -519,14 +580,16 @@
             jax.ShapeDtypeStruct((lines, width), F32),
             jax.ShapeDtypeStruct((toks, width), F32),
         ],
-        in_specs=[vmem] * 12 + [anyw] * 3,
+        in_specs=[vmem] * 11 + [anyw] * 3,
         out_specs=[anyw] * 3 + [vmem] * 2,
         scratch_shapes=[
             pltpu.VMEM((2, half, width), BF16),
             pltpu.VMEM((2, 2 * half, feats), BF16),
             pltpu.VMEM((3, units, feats), BF16),
-            pltpu.VMEM((3, units, 2 * half), F32),
-            pltpu.VMEM((3, units, 2 * half), BF16),
+            pltpu.VMEM((3, feats, units), BF16),
+            pltpu.VMEM((3, 2 * half, units), F32),
+            pltpu.VMEM((3, 2 * half, units), BF16),
+            pltpu.VMEM((units, 2 * half), BF16),
             pltpu.VMEM((half, feats), BF16),
             pltpu.VMEM((half, feats), BF16),
             pltpu.VMEM((half, feats), BF16),
@@ -537,7 +600,6 @@
             pltpu.VMEM((half, width), BF16),
             pltpu.VMEM((toks, feats), BF16),
             pltpu.VMEM((toks, feats), BF16),
-            pltpu.VMEM((3, units, feats), BF16),
             pltpu.VMEM((nz, nx, 2, lines, width), BF16),
             pltpu.VMEM((nx, 2, toks, width), BF16),
             pltpu.VMEM((nz, 2 * nx, lines, toks), BF16),
@@ -550,8 +612,9 @@
             pltpu.VMEM((plane, lanes, 128), F32),
             pltpu.VMEM((plane, lanes, 128), F32),
             pltpu.VMEM((2, lanes, 128), F32),
-            dma, dma((3,)), dma((3,)),
-            dma, dma((nz,)), dma((2, nz)), dma((2, nz)), dma((nz,)), dma((nz,)), dma, dma,
+            pltpu.VMEM((toks, half), BF16),
+            dma((3,)), dma((3,)),
+            dma, dma((nz,)), dma((2, nz)), dma((2, nz)), dma((nz,)), dma((nz,)), dma, dma((2, 4)),
             dma((nz // 2,)), dma((nz // 2,)), dma((6, nz // 2)), dma((6, nz // 2)), dma, dma,
             dma((3,)), dma((3,)), dma((nx - 1,)), dma((nx - 1,)), dma((2, nz // 2)),
             dma((2, nz // 2)), dma, dma, dma((nx - 1,)), dma((nx - 1,)), dma, dma, dma((2,)),
@@ -580,29 +643,23 @@
     memory_switch_tiles,
     entry_switch_tiles,
 ):
-    tok_rows, feature_count = result_cotangent_values.shape
-    route_count = chosen_specialists.shape[1]
+    tok_rows = result_cotangent_values.shape[0]
     sp_count = lax.axis_size(SP)
     expert_count = sp_count // SLICES
     capacity = min(tok_rows, 4 * tok_rows // expert_count)
-    pairs = chosen_specialists.T.reshape(-1)
-    order = (jnp.arange(tok_rows)[None, :] * route_count + jnp.arange(route_count)[:, None]).reshape(-1)
-    earlier = (pairs[:, None] == pairs[None, :]) & (order[:, None] < order[None, :])
-    target = pairs * capacity + jnp.sum(earlier.astype(jnp.int32), axis=0)
     dims = (lax.axis_size("sp_0"), lax.axis_size("sp_1"), lax.axis_size("tp"))
     gate_weight_grad, up_weight_grad, down_grad, out_proj_grad, lru_input_grad = layer(
         dims,
         capacity,
-        target[None, :],
-        target.reshape(route_count, tok_rows).T,
-        specialist_mixing_shares,
+        chosen_specialists.T,
+        specialist_mixing_shares.T,
         result_cotangent_values,
         specialist_entry_vectors,
         memory_readout_map,
         memory_source_vectors,
         memory_hidden_values,
         feature_fading_speed[None, :],
-        extra_log_fading[:, None],
+        extra_log_fading[None, :],
         memory_switch_tiles,
         entry_switch_tiles,
         specialist_switch_maps[0].T,

time: 152 us -> 136 us (0.89)
  Pallas kernels: 138 us -> 127 us
  local copies, waits for them, and re-layouts: 11.6 us -> 7.8 us
    pallas_call x1, Pallas kernels: 138 us -> 127 us  [layer(): pl.pallas_call(functools.partial(layer_entry, dims, cap), out_shape=[jax....]
    unnamed x15 -> x13, local copies, waits for them, and re-layouts: 10 us -> 7.8 us
where the time goes in v3:
time: 136 us; the launch traced here: 135 us
  Pallas kernels  127 us (93%)
  local copies, waits for them, and re-layouts  7.8 us (6%)
    pallas_call x1, Pallas kernels, layer(): pl.pallas_call(functools.partial(layer_entry, dims, cap), out_shape=[jax....  127 us
    unnamed x13, local copies, waits for them, and re-layouts  7.8 us

profile of v3, /device:TPU:1, one launch (start us, length us, event | category | flops | bytes accessed | tf_op | source)
XLA Modules:
  0.0 135.4 jit_solution(7049465817763889585)
XLA Ops:
  0.6 126.9 %layer.1 = (bf16[448,2048]{1,0:T(8,128)(2,1)}, bf16[448,2048]{1,0:T(8,128)(2,1)}, bf16[448,2048]{1,0:T(8,128)(2,1)}, f32[32,512]{1,0:T(8,128)}, f32[128,512]{1,0:T(8,128)}) custom-call(s32[2,128]{1,0:T(2,128)} %bitcast.25, f32[2,128]{1,0:T(2,128)} %bitcast.26, bf16[128,2048]{1,0:T(8,128)(2,1)} %refs_2_.1, bf16[128,2048]{1,0:T(8,128)(2,1)} %refs_3_.1, ...), custom_call_target="tpu_custom_call" | custom-call | tf_op jit(solution)/shard_map/layer/pallas_call | solution.py:576
  127.6 0.0 copy-start.1
  127.6 3.1 %copy.24 = bf16[1,2048,448]{1,2,0:T(8,128)(2,1)} copy(bf16[1,2048,448]{1,2,0:T(8,128)(2,1)} %bitcast.20) | data formatting | bytes 3670016
  130.7 0.0 copy-done.1
  130.7 0.0 copy-start
  130.7 1.2 copy.25
  131.9 0.9 copy-done
  132.8 0.0 copy-start.3
  132.8 0.0 copy-start.2
  132.8 1.2 copy.26
  134.1 0.0 copy-done.3
  134.1 0.6 copy.27
  134.7 0.0 copy-done.2
  134.7 0.7 copy.28
Async XLA Ops:
  127.6 3.1 %copy-start.1 = (bf16[448,2048]{1,0:T(8,128)(2,1)S(1)}, bf16[448,2048]{1,0:T(8,128)(2,1)}, u32[]{:S(2)}) copy-start(bf16[448,2048]{1,0:T(8,128)(2,1)} %get-tuple-element.11) | copy-start | bytes 5505028
  130.7 2.2 %copy-start = (bf16[448,2048]{1,0:T(8,128)(2,1)S(1)}, bf16[448,2048]{1,0:T(8,128)(2,1)}, u32[]{:S(2)}) copy-start(bf16[448,2048]{1,0:T(8,128)(2,1)} %get-tuple-element.12) | copy-start | bytes 5505028
  132.8 1.2 copy-start.3
  132.8 1.9 %copy-start.2 = (f32[128,512]{1,0:T(8,128)S(1)}, f32[128,512]{1,0:T(8,128)}, u32[]{:S(2)}) copy-start(f32[128,512]{1,0:T(8,128)} %get-tuple-element.24) | copy-start | bytes 786436

commit v4 on v3

--- a/solution.py
+++ b/solution.py
@@ -111,11 +111,15 @@
     def source(e):
         return slots.at[:, pl.ds(pl.multiple_of(e * cap, cap), cap), :]
 
+    mid, piece = nz // 2, half // 2
+
+    def row_of(side, k):
+        return (k // mid) * half + side * piece + (k % mid) * group
+
     def landing(k):
-        start = pl.multiple_of(c * half + (k * nx + x) * cap, cap)
-        return xy.at[:, pl.ds(start, cap), cols(0)]
-
-    here = pl.ds(pl.multiple_of(c * half + x * cap, cap), cap)
+        return xy.at[:, pl.ds(pl.multiple_of(row_of(c, k) + x * cap, cap), cap), cols(0)]
+
+    here = pl.ds(pl.multiple_of(row_of(c, 0) + x * cap, cap), cap)
     mine_too = pl.ds(pl.multiple_of(me * cap, cap), cap)
     for i in range(2):
         xy[i, here, cols(0)] = slots[i, mine_too, :]
@@ -130,8 +134,7 @@
         lax.fori_loop(1 if k == 0 else 0, nx, one, 0)
 
     ahead = 3
-    for k in range(ahead):
-        push(k)
+    push(0)
 
     def push_rest():
         for step in range(1, nx):
@@ -227,17 +230,15 @@
         lax.fori_loop(0, plane, weigh, jnp.ones((width // 128, 128), F32))
 
     def block(k, turn):
-        start = pl.multiple_of(c * half + k * group, cap)
-        return xy.at[:, pl.ds(start, group), cols(turn)]
+        return xy.at[:, pl.ds(pl.multiple_of(row_of(c, k), cap), group), cols(turn)]
 
     def across(k, turn):
-        remote(block(k, turn), block(k, turn), c_send, c_recv.at[k // (nz // 2), turn], other)
+        remote(block(k, turn), block(k, turn), c_send, c_recv.at[k // mid, turn], other)
 
     def along(k, turn, to, send, recv):
         remote(block(k, turn), block(k, turn), send, recv, to)
 
     turn_dims = (((1,), (1,)), ((), ()))
-    piece = half // 2
     units = accs.shape[2]
 
     def flip(m):
@@ -250,17 +251,22 @@
 
         lax.fori_loop(0, feats // 128, some, 0)
 
-    def forward(own, part, turn):
-        side = c if own else 1 - c
-        here = pl.ds(pl.multiple_of(side * half + part * piece, cap), piece)
-        if not own:
-            drained(xy.at[:, here, cols(turn)], c_recv.at[part, turn])
+    def forward(part, turns):
+        here = pl.ds(part * half, half)
+        theirs = pl.ds(pl.multiple_of(part * half + (1 - c) * piece, cap), piece)
+        for turn in turns:
+            drained(xy.at[:, theirs, cols(turn)], c_recv.at[part, turn])
 
         def some(m, _):
-            got = jnp.dot(
-                xy[m // 2, here, cols(turn)], flipped[m, cols(turn), :], preferred_element_type=F32
+            got = sum(
+                jnp.dot(
+                    xy[m // 2, here, cols(turn)],
+                    flipped[m, cols(turn), :],
+                    preferred_element_type=F32,
+                )
+                for turn in turns
             )
-            if turn == 0:
+            if 0 in turns:
                 accs[m, here, :] = got
             else:
                 accs[m, here, :] += got
@@ -272,8 +278,7 @@
         tile = 16
 
         def some(i, _):
-            side, n = i // (piece // tile), lax.rem(i, piece // tile)
-            here = pl.ds(pl.multiple_of(side * half + part * piece + n * tile, tile), tile)
+            here = pl.ds(pl.multiple_of(part * half + i * tile, tile), tile)
             gate, wider, backed = accs[0, here, :], accs[1, here, :], accs[2, here, :]
             sig = jax.nn.sigmoid(gate)
             active = gate * sig
@@ -282,7 +287,7 @@
             acts[2, here, :] = (active * wider).astype(BF16)
             return 0
 
-        lax.fori_loop(0, 2 * (piece // tile), some, 0)
+        lax.fori_loop(0, half // tile, some, 0)
 
     chunk = 2 * group
     chunks = nz // 2
@@ -290,7 +295,7 @@
     def step_rows(i):
         at = i * chunk
         lines = [
-            pl.ds(pl.multiple_of(side * half + at, chunk), chunk) for side in (1 - c, c)
+            pl.ds(pl.multiple_of(row_of(side, 2 * i), chunk), chunk) for side in (1 - c, c)
         ]
         left = [jnp.concatenate([acts[m, n, :] for n in lines], axis=0) for m in range(2)]
 
@@ -402,23 +407,22 @@
     def work(what, *args):
         return functools.partial(what, *args)
 
-    mid = nz // 2
     fillers = {}
     for at, jobs in (
-        (0, [work(flip, 0), work(flip, 2)]),
-        (1, [work(flip, 1), work(gates)]),
-        (2, [work(products)]),
+        (0, [work(flip, 2)]),
+        (1, [work(flip, 1)]),
+        (2, [work(gates), work(products)]),
         (3, [work(push_rest)]),
-        (mid, [work(forward, True, 0, 0)]),
-        (mid + 1, [work(forward, False, 0, 0), work(forward, True, 0, 3)]),
-        (mid + 2, [work(forward, True, 0, 1), work(forward, False, 0, 3)]),
-        (mid + 3, [work(forward, True, 0, 2), work(forward, False, 0, 1)]),
-        (nz, [work(forward, False, 0, 2), work(ring, 0), work(forward, True, 1, 0)]),
-        (nz + 1, [work(activate, 0), work(hand_over), work(step_rows, 0),
-                  work(forward, False, 1, 0), work(forward, True, 1, 3)]),
-        (nz + 2, [work(step_rows, 1), work(forward, True, 1, 1), work(forward, False, 1, 3)]),
+        (mid + 1, [work(forward, 0, (0,))]),
+        (mid + 3, [work(forward, 0, (1, 3))]),
+        (nz, [work(forward, 0, (2,)), work(ring, 0)]),
+        (nz + 1, [work(activate, 0), work(step_rows, 0), work(forward, 1, (0,))]),
+        (nz + 2, [work(step_rows, 1), work(hand_over), work(ring, 1)]),
     ):
         fillers.setdefault(at, []).extend(jobs)
+    flip(0)
+    for k in range(1, ahead):
+        push(k)
     for turn in range(nz + 3):
         if turn < nz:
             receive(turn)
@@ -428,34 +432,28 @@
             receive_far(turn - 3)
         for job in fillers.get(turn, []):
             job()
-    receive_far(nz - 1)
     early = chunks // 2
     for i in range(early):
         step_pair(i)
-    ring(1)
-    forward(False, 1, 1)
-    forward(True, 1, 2)
-    forward(False, 1, 2)
+    forward(1, (1, 3))
+    receive_far(nz - 1)
+    forward(1, (2,))
     activate(1)
-    later_rings = list(range(2, rounds + 1))
     for i in range(early):
         step_rows(early + i)
         step_far(i)
     for i in range(early):
         step_pair(early + i)
         step_near(i)
-    if later_rings:
-        ring(later_rings.pop(0))
+    ring(2)
     for i in range(early):
         step_far(early + i)
     for i in range(early):
-        if later_rings:
-            ring(later_rings.pop(0))
         step_near(early + i)
     weight_grad(0)
-    for s in later_rings:
-        ring(s)
     weigh_all()
+    if rounds > 2:
+        ring(3)
 
     drained(back.at[pl.ds(0, half - cap), :], r_recv)
     moe[:, cols(0)] = jnp.dot(picked[...], back[...], preferred_element_type=F32).astype(BF16)
@@ -465,6 +463,8 @@
             (z, x, c, lax.rem(y + step, ny)),
         )
     weight_grad(1)
+    for s in range(4, rounds + 1):
+        ring(s)
     drained(wide.at[:, :, 1 - c], s_recv)
     drained(held.at[:, 1 - c], t_recv)
     for step in (1, 3, 2):
@@ -472,16 +472,19 @@
     mixed[...] = (cot[...].astype(F32) + moe[...].astype(F32)).astype(BF16)
 
     lines = rmap.shape[0]
-    turned[...] = jnp.transpose(mixed[...]).reshape(nz, 2 * nx, lines, toks)
+    across_mixed = jnp.transpose(mixed[...]).reshape(nz, 2 * nx, lines, toks)
+    for i in range(nz):
+        turned[i % 2, i // 2] = across_mixed[i]
     spot = x * 2 + c
     ours = pl.ds(pl.multiple_of(spot * toks, toks), toks)
-    cross[:, :, ours] = turned[:, spot]
-    for step in range(1, 2 * nx):
-        to = lax.rem(spot + step, 2 * nx)
-        remote(
-            turned.at[:, to], cross.at[:, :, ours], g_send.at[step - 1], g_recv.at[step - 1],
-            (z, to // 2, lax.rem(to, 2), y),
-        )
+    cross[:, :, :, ours] = turned[:, :, spot]
+    for odd in range(2):
+        for step in range(1, 2 * nx):
+            to = lax.rem(spot + step, 2 * nx)
+            remote(
+                turned.at[odd, :, to], cross.at[odd, :, :, ours], g_send.at[odd, step - 1],
+                g_recv.at[odd, step - 1], (z, to // 2, lax.rem(to, 2), y),
+            )
 
     state = jnp.dot(mixed[...], wide[...].reshape(-1, width), preferred_element_type=F32)
     for n, s in enumerate(reach):
@@ -492,18 +495,29 @@
     alphas[index] = small[1]
     tell(small.at[1], alphas, a_send.at[1], a_recv.at[1])
 
-    for step in range(1, 2 * nx):
-        drained(turned.at[:, 0], g_recv.at[step - 1])
-    total = jnp.dot(
-        cross[...].reshape(nz * lines, 2 * nx * toks),
-        held[...].reshape(2 * nx * toks, width),
-        preferred_element_type=F32,
-    )
-    fold[...] = total.astype(BF16).reshape(nz, lines, width)
+    def fold_in(odd):
+        for step in range(1, 2 * nx):
+            drained(turned.at[0, :, 0], g_recv.at[odd, step - 1])
+        total = jnp.dot(
+            cross[odd].reshape(mid * lines, 2 * nx * toks),
+            held[...].reshape(2 * nx * toks, width),
+            preferred_element_type=F32,
+        )
+        total = total.astype(BF16).reshape(mid, lines, width)
+        for i in range(mid):
+            fold[2 * i + odd] = total[i]
+        for step in range(1, nz):
+            to = lax.rem(z + step, nz)
+
+            @pl.when(lax.rem(to, 2) == odd)
+            def _():
+                remote(
+                    fold.at[to], rest.at[z], q_send.at[step - 1], q_recv.at[step - 1], (to, x, c, y)
+                )
+
+    fold_in(0)
+    fold_in(1)
     rest[z] = fold[z]
-    for step in range(1, nz):
-        to = lax.rem(z + step, nz)
-        remote(fold.at[to], rest.at[z], q_send.at[step - 1], q_recv.at[step - 1], (to, x, c, y))
 
     drained(alphas.at[pl.ds(0, plane - 1)], a_recv.at[1])
     carried = jnp.sum(weights[...] * alphas[...], axis=0)
@@ -528,8 +542,7 @@
         summed = summed + rest[i].astype(F32)
     proj_out[...] = summed
 
-    whole = xy.at[:, pl.ds(pl.multiple_of(c * half, cap), half), :]
-    drained(whole, c_send)
+    drained(xy.at[:, pl.ds(0, half), :], c_send)
     drained(slots.at[:, pl.ds(0, half - cap), :], d_send)
     for k in range(nz):
         drained(block(k, 0), y_send.at[0, k])
@@ -553,7 +566,8 @@
     for i in range(2):
         drained(betas.at[pl.ds(0, plane - 1)], a_send.at[i])
     for step in range(2 * nx - 1):
-        drained(turned.at[:, 0], g_send.at[step])
+        for odd in range(2):
+            drained(turned.at[0, :, 0], g_send.at[odd, step])
     for step in range(nz - 1):
         drained(fold.at[0], q_send.at[step])
     for m in range(3):
@@ -602,8 +616,8 @@
             pltpu.VMEM((toks, feats), BF16),
             pltpu.VMEM((nz, nx, 2, lines, width), BF16),
             pltpu.VMEM((nx, 2, toks, width), BF16),
-            pltpu.VMEM((nz, 2 * nx, lines, toks), BF16),
-            pltpu.VMEM((nz, lines, 2 * nx * toks), BF16),
+            pltpu.VMEM((2, nz // 2, 2 * nx, lines, toks), BF16),
+            pltpu.VMEM((2, nz // 2, lines, 2 * nx * toks), BF16),
             pltpu.VMEM((nz, lines, width), BF16),
             pltpu.VMEM((nz, lines, width), BF16),
             pltpu.VMEM((steps, toks, width), F32),
@@ -618,13 +632,52 @@
             dma((nz // 2,)), dma((nz // 2,)), dma((6, nz // 2)), dma((6, nz // 2)), dma, dma,
             dma((3,)), dma((3,)), dma((nx - 1,)), dma((nx - 1,)), dma((2, nz // 2)),
             dma((2, nz // 2)), dma, dma, dma((nx - 1,)), dma((nx - 1,)), dma, dma, dma((2,)),
-            dma((2,)), dma((2 * nx - 1,)), dma((2 * nx - 1,)), dma((nz - 1,)), dma((nz - 1,)),
+            dma((2,)), dma((2, 2 * nx - 1)), dma((2, 2 * nx - 1)), dma((nz - 1,)), dma((nz - 1,)),
         ],
         compiler_params=pltpu.CompilerParams(
             collective_id=0, has_side_effects=True, vmem_limit_bytes=60 * 2**20
         ),
         name="layer",
     )(*operands)
+
+
+def settle_kernel(arrays, parts, *refs):
+    ins, outs, held = refs[:arrays], refs[arrays : 2 * arrays], refs[2 * arrays : 3 * arrays]
+    in_sem, out_sem = refs[3 * arrays :]
+    jobs, n = [], 0
+    for i in range(arrays):
+        for part in range(parts[i]):
+            tall = ins[i].shape[0] // parts[i]
+            some = pl.ds(part * tall, tall)
+            jobs.append(
+                (
+                    pltpu.make_async_copy(ins[i].at[some], held[i].at[some], in_sem.at[n]),
+                    pltpu.make_async_copy(held[i].at[some], outs[i].at[some], out_sem.at[n]),
+                )
+            )
+            n += 1
+    for first, _ in jobs:
+        first.start()
+    for first, second in jobs:
+        first.wait()
+        second.start()
+    for _, second in jobs:
+        second.wait()
+
+
+def settled(arrays):
+    parts = [4 if a.dtype == BF16 else 1 for a in arrays]
+    anyw, dma = pl.BlockSpec(memory_space=pl.ANY), pltpu.SemaphoreType.DMA
+    return pl.pallas_call(
+        functools.partial(settle_kernel, len(arrays), parts),
+        out_shape=[jax.ShapeDtypeStruct(a.shape, a.dtype) for a in arrays],
+        in_specs=[anyw] * len(arrays),
+        out_specs=[anyw] * len(arrays),
+        scratch_shapes=[pltpu.VMEM(a.shape, a.dtype) for a in arrays]
+        + [dma((sum(parts),)), dma((sum(parts),))],
+        compiler_params=pltpu.CompilerParams(vmem_limit_bytes=60 * 2**20),
+        name="settle",
+    )(*arrays)
 
 
 def local(
@@ -648,7 +701,7 @@
     expert_count = sp_count // SLICES
     capacity = min(tok_rows, 4 * tok_rows // expert_count)
     dims = (lax.axis_size("sp_0"), lax.axis_size("sp_1"), lax.axis_size("tp"))
-    gate_weight_grad, up_weight_grad, down_grad, out_proj_grad, lru_input_grad = layer(
+    gate_weight_grad, up_weight_grad, down_grad, out_proj_grad, lru_input_grad = settled(layer(
         dims,
         capacity,
         chosen_specialists.T,
@@ -665,7 +718,7 @@
         specialist_switch_maps[0].T,
         specialist_widen_maps[0].T,
         specialist_shrink_maps[0],
-    )
+    ))
     return (
         gate_weight_grad.T[None],
         up_weight_grad.T[None],

time: 136 us -> 129 us (0.949); the launches traced: 135 us -> 127 us
  local copies, waits for them, and re-layouts: 7.8 us -> 0 us
    unnamed x13 -> x0, local copies, waits for them, and re-layouts: 7.8 us -> none
    pallas_call x1, Pallas kernels: 127 us -> 121 us  [layer(): pl.pallas_call(functools.partial(layer_entry, dims, cap), out_shape=[jax....]
    pallas_call x0 -> x1, Pallas kernels: none -> 5.23 us  [settled(): pl.pallas_call(functools.partial(settle_kernel, len(arrays), parts), out_...]
where the time goes in v4:
time: 129 us; the launch traced here: 127 us
  Pallas kernels  126 us (98%)
    pallas_call x1, Pallas kernels, layer(): pl.pallas_call(functools.partial(layer_entry, dims, cap), out_shape=[jax....  121 us
    pallas_call x1, Pallas kernels, settled(): pl.pallas_call(functools.partial(settle_kernel, len(arrays), parts), out_...  5.23 us

profile of v4, /device:TPU:1, one launch (start us, length us, event | category | flops | bytes accessed | tf_op | source)
XLA Modules:
  0.0 126.9 jit_solution(6705734955079001724)
XLA Ops:
  0.6 121.0 %layer.1 = (bf16[448,2048]{1,0:T(8,128)(2,1)}, bf16[448,2048]{1,0:T(8,128)(2,1)}, bf16[448,2048]{1,0:T(8,128)(2,1)}, f32[32,512]{1,0:T(8,128)}, f32[128,512]{1,0:T(8,128)}) custom-call(s32[2,128]{1,0:T(2,128)} %bitcast.22, f32[2,128]{1,0:T(2,128)} %bitcast.23, bf16[128,2048]{1,0:T(8,128)(2,1)} %refs_2_.1, bf16[128,2048]{1,0:T(8,128)(2,1)} %refs_3_.1, ...), custom_call_target="tpu_custom_call" | custom-call | tf_op jit(solution)/shard_map/layer/pallas_call | solution.py:590
  121.7 5.2 %settle.1 = (bf16[448,2048]{1,0:T(8,128)(2,1)}, bf16[448,2048]{1,0:T(8,128)(2,1)}, bf16[448,2048]{1,0:T(8,128)(2,1)}, f32[32,512]{1,0:T(8,128)}, f32[128,512]{1,0:T(8,128)}) custom-call(bf16[448,2048]{1,0:T(8,128)(2,1)} %get-tuple-element.15.refs_0_, bf16[448,2048]{1,0:T(8,128)(2,1)} %get-tuple-element.16.refs_1_, ...), custom_call_target="tpu_custom_call" | custom-call | tf_op jit(solution)/shard_map/settle/pallas_call | solution.py:671

commit v5 on v4

--- a/solution.py
+++ b/solution.py
@@ -133,7 +133,7 @@
 
         lax.fori_loop(1 if k == 0 else 0, nx, one, 0)
 
-    ahead = 3
+    ahead = 5
     push(0)
 
     def push_rest():

time: 129 us -> 127 us (0.984); the launches traced: 127 us -> 127 us
  no operation moved by 1% of the time
where the time goes in v5:
time: 127 us
  Pallas kernels  126 us (99%)
    pallas_call x1, Pallas kernels, layer(): pl.pallas_call(functools.partial(layer_entry, dims, cap), out_shape=[jax....  121 us
    pallas_call x1, Pallas kernels, settled(): pl.pallas_call(functools.partial(settle_kernel, len(arrays), parts), out_...  5.23 us

profile of v5, /device:TPU:1, one launch (start us, length us, event | category | flops | bytes accessed | tf_op | source)
XLA Modules:
  0.0 126.8 jit_solution(8703297468747054131)
XLA Ops:
  0.6 120.9 %layer.1 = (bf16[448,2048]{1,0:T(8,128)(2,1)}, bf16[448,2048]{1,0:T(8,128)(2,1)}, bf16[448,2048]{1,0:T(8,128)(2,1)}, f32[32,512]{1,0:T(8,128)}, f32[128,512]{1,0:T(8,128)}) custom-call(s32[2,128]{1,0:T(2,128)} %bitcast.22, f32[2,128]{1,0:T(2,128)} %bitcast.23, bf16[128,2048]{1,0:T(8,128)(2,1)} %refs_2_.1, bf16[128,2048]{1,0:T(8,128)(2,1)} %refs_3_.1, ...), custom_call_target="tpu_custom_call" | custom-call | tf_op jit(solution)/shard_map/layer/pallas_call | solution.py:590
  121.6 5.2 %settle.1 = (bf16[448,2048]{1,0:T(8,128)(2,1)}, bf16[448,2048]{1,0:T(8,128)(2,1)}, bf16[448,2048]{1,0:T(8,128)(2,1)}, f32[32,512]{1,0:T(8,128)}, f32[128,512]{1,0:T(8,128)}) custom-call(bf16[448,2048]{1,0:T(8,128)(2,1)} %get-tuple-element.15.refs_0_, bf16[448,2048]{1,0:T(8,128)(2,1)} %get-tuple-element.16.refs_1_, ...), custom_call_target="tpu_custom_call" | custom-call | tf_op jit(solution)/shard_map/settle/pallas_call | solution.py:671
